TPU v7x, 512 devices: a whole 4x4x16 slice. The times are simulated.
512 devices in a mesh: sp: 16 (over z), tp: 32 (over y, x, core).
Axes of the slice: x: 4, y: 4, z: 16, core: 2. Of those that a mesh axis runs over, the one named last changes fastest.
Arguments:
- target: bfloat16 [2048, 2048], P('sp'), may hold values from -6 to 6
- source: bfloat16 [4096, 2048], P(('sp', 'tp')), may hold values from -6 to 6
- cotangent: bfloat16 [2048, 2048], P('sp'), may hold values from -6 to 6
- target_gain: float32 [2048], replicated, may hold values from 0.1 to 1.9
- source_gain: float32 [2048], replicated, may hold values from 0.1 to 1.9
- query_weight: bfloat16 [2048, 8192], P(None, 'tp'), may hold values from -4 to 4
- key_weight: bfloat16 [2048, 2048], P(None, 'tp'), may hold values from -1 to 1
- value_projection_weight: bfloat16 [2048, 2048], P(None, 'tp'), may hold values from -0.125 to 0.125
- output_weight: bfloat16 [8192, 2048], P('tp'), may hold values from -0.0625 to 0.0625
Outputs:
- target_grad: float32 [2048, 2048], P(('sp', 'tp'))
- source_grad: float32 [4096, 2048], P(('sp', 'tp'))
- key_weight_grad: float32 [2048, 2048], P(None, 'tp')
All inputs are finite; a program needn't handle non-finite values.
Results may differ from a plain program's by a relative error of at most 0.018.
The roundings to bfloat16 on the way count: a program that leaves them out, or rounds other values in their place, can miss the bound.
Values may be sent and summed in bfloat16 or wider, within the bound.
A program may use at most 64 MiB of HBM per device.

v0:
```python
import jax
import jax.numpy as jnp
from jax import lax
from jax.sharding import PartitionSpec as P

HEAD_SIZE = 256


EPSILON = 1e-05


def partner_2(value, axis, bit):
    mask = 2**bit
    pairs = [(source, source ^ mask) for source in range(lax.axis_size(axis))]
    return lax.ppermute(value, axis, pairs)


def from_everyone(array, axis):
    copies = jnp.broadcast_to(array, (lax.axis_size(axis), *array.shape))
    return lax.all_to_all(copies, axis, split_axis=0, concat_axis=0, tiled=True)


def joined_along(tiles, dim):
    tiles = jnp.moveaxis(tiles, 0, dim)
    lengths = tiles.shape
    return tiles.reshape(*lengths[:dim], lengths[dim] * lengths[dim + 1], *lengths[dim + 2 :])


def gather_directly(array, axis, dim):
    tiles = from_everyone(array, axis)
    return joined_along(tiles, dim)


def side_by_side(arrays, axis, dim, along):
    both = jnp.concatenate(arrays, axis=along)
    out, at, gathered = (lax.all_gather(both, axis, axis=dim, tiled=True), 0, [])
    for a in arrays:
        gathered.append(lax.slice_in_dim(out, at, at + a.shape[along], axis=along))
        at += a.shape[along]
    return tuple(gathered)


def all_in_one(array, axis):
    leaves = jax.tree.leaves(array)
    sequence = sorted(range(len(leaves)), key=lambda k: -leaves[k].size)
    width = (1, *leaves[sequence[0]].shape)[-1]
    lines = [
        jnp.pad(leaves[k].reshape(-1), (0, -leaves[k].size % width)).reshape(-1, width)
        for k in sequence
    ]
    both, at, found = (from_everyone(jnp.concatenate(lines), axis), 0, {})
    for k, line in zip(sequence, lines):
        piece = both[:, at : at + len(line)].reshape(len(both), -1)
        found[k] = piece[:, : leaves[k].size].reshape(-1, *leaves[k].shape)
        at += len(line)
    numbers = iter(range(len(leaves)))
    return jax.tree.map(lambda _: found[next(numbers)], array)


def combined_pairwise(pieces, combine):
    while len(jax.tree.leaves(pieces)[0]) > 1:
        pieces = jax.vmap(combine)(
            *(jax.tree.map(lambda part: part[side::2], pieces) for side in (0, 1))
        )
    return jax.tree.map(lambda part: part[0], pieces)


def merged(array, axis, combine):
    pieces = all_in_one(array, axis)
    return combined_pairwise(pieces, combine)


def gathered_total(array, axis):
    return lax.all_gather(array, axis).astype(jnp.float32).sum(0)


def cut_along(array, dim, devices):
    before, after = (array.shape[:dim], array.shape[dim + 1 :])
    return jnp.moveaxis(array.reshape(*before, devices, -1, *after), dim, 0)


def summed_on_arrival(array, axis, dim):
    devices = lax.axis_size(axis)
    tiles = lax.all_to_all(cut_along(array, dim, devices), axis, 0, 0, tiled=True)
    return jnp.sum(tiles.astype(jnp.float32), axis=0)


def sent_and_summed(array, axis, dim):
    devices = lax.axis_size(axis)
    tiles = lax.all_to_all(cut_along(array, dim, devices), axis, 0, 0, tiled=True)
    return jnp.sum(tiles, axis=0)


def norm_rows(rows):
    values = rows.astype(jnp.float32)
    centred = values - jnp.mean(values, axis=-1, keepdims=True)
    inverse = lax.rsqrt(jnp.mean(centred * centred, axis=-1, keepdims=True) + EPSILON)
    return (centred * inverse, inverse)


def norm_back(scaled, inverse, gain, upstream):
    weighted = upstream * gain
    spread = jnp.mean(weighted * scaled, axis=-1, keepdims=True)
    return inverse * (weighted - jnp.mean(weighted, axis=-1, keepdims=True) - scaled * spread)


def times_transposed(left, right):
    return lax.dot_general(
        left, right, (((1,), (1,)), ((), ())), preferred_element_type=jnp.float32
    )


def split_heads(flat):
    return flat.reshape(flat.shape[0], flat.shape[1] // HEAD_SIZE, HEAD_SIZE)


def head_scores(queries, key_rows):
    return jnp.einsum(
        "rhd,sd->hrs", queries, key_rows, preferred_element_type=jnp.float32
    ) * HEAD_SIZE ** (-0.5)


def block_statistics(queries, out_grads, key_rows, value_rows):
    scores = head_scores(queries, key_rows)
    highest = jnp.max(scores, axis=2)
    weights = jnp.exp(scores - highest[:, :, None])
    products = jnp.einsum("rhd,sd->hrs", out_grads, value_rows, preferred_element_type=jnp.float32)
    return (highest, jnp.sum(weights, axis=2), jnp.sum(weights * products, axis=2))


def combine_statistics(former, latter):
    highest = jnp.maximum(former[0], latter[0])
    early_scale = jnp.exp(former[0] - highest)
    late_scale = jnp.exp(latter[0] - highest)
    return (
        highest,
        former[1] * early_scale + latter[1] * late_scale,
        former[2] * early_scale + latter[2] * late_scale,
    )


def score_grads(queries, out_grads, key_rows, value_rows, log_total, drifts):
    scores = head_scores(queries, key_rows)
    softmax_weights = jnp.exp(scores - log_total[:, :, None])
    products = jnp.einsum("rhd,sd->hrs", out_grads, value_rows, preferred_element_type=jnp.float32)
    slopes = (softmax_weights * (products - drifts[:, :, None]) * HEAD_SIZE ** (-0.5)).astype(
        jnp.bfloat16
    )
    return (softmax_weights.astype(jnp.bfloat16), slopes)


def join_heads(stacked):
    position = lax.axis_index("tp")
    part_cols = stacked.shape[2]
    bit_level = 0
    while part_cols < HEAD_SIZE:
        partner = partner_2(stacked, "tp", bit_level)
        upper_half = position >> bit_level & 1
        stacked = jnp.where(
            upper_half == 0,
            jnp.concatenate((stacked, partner), 2),
            jnp.concatenate((partner, stacked), 2),
        )
        part_cols = part_cols * 2
        bit_level = bit_level + 1
    return stacked


def split_sums(stacked, part_cols):
    position = lax.axis_index("tp")
    bit_count = (HEAD_SIZE // part_cols).bit_length() - 1
    for bit_level in reversed(range(bit_count)):
        half_cols = stacked.shape[2] // 2
        lower_half = stacked[:, :, :half_cols]
        upper_cols = stacked[:, :, half_cols:]
        upper_half = position >> bit_level & 1
        kept_half = jnp.where(upper_half == 0, lower_half, upper_cols)
        sent_half = jnp.where(upper_half == 0, upper_cols, lower_half)
        stacked = kept_half + partner_2(sent_half, "tp", bit_level)
    return stacked


def on_device(
    target,
    source,
    cotangent,
    target_gain,
    source_gain,
    query_weight,
    key_weight,
    value_projection_weight,
    output_weight,
):
    part_cols = key_weight.shape[1]
    src_scaled, src_inverse = norm_rows(source)
    src_normed = (src_scaled * source_gain).astype(jnp.bfloat16)
    tgt_scaled, tgt_inverse = norm_rows(target)
    tgt_normed = (tgt_scaled * target_gain).astype(jnp.bfloat16)
    block_rows = gather_directly(src_normed, "tp", 0)
    key_portion = jnp.dot(block_rows, key_weight, preferred_element_type=jnp.float32).astype(
        jnp.bfloat16
    )
    value_part = jnp.dot(
        block_rows, value_projection_weight, preferred_element_type=jnp.float32
    ).astype(jnp.bfloat16)
    parted = jnp.stack((key_portion, value_part))
    queries = split_heads(
        jnp.dot(tgt_normed, query_weight, preferred_element_type=jnp.float32).astype(jnp.bfloat16)
    )
    out_grads = split_heads(times_transposed(cotangent, output_weight).astype(jnp.bfloat16))
    head_count = queries.shape[1]
    own_rows = queries.shape[0]
    own_keys = join_heads(parted)
    pieces = side_by_side((queries, out_grads), "sp", 0, 1)
    fresh_stats = block_statistics(pieces[0], pieces[1], own_keys[0], own_keys[1])
    partial_value = tuple((fresh for fresh in fresh_stats))
    highest, totals, weighted = merged(partial_value, "sp", combine_statistics)
    log_total = highest + jnp.log(totals)
    drifts = weighted / totals
    pieces = side_by_side((queries, out_grads), "sp", 0, 1)
    attention, slopes = score_grads(
        pieces[0], pieces[1], own_keys[0], own_keys[1], log_total, drifts
    )
    key_gradient_rows = jnp.einsum(
        "hrs,rhd->sd", slopes, pieces[0], preferred_element_type=jnp.float32
    )
    value_gradient_rows = jnp.einsum(
        "hrs,rhd->sd", attention, pieces[1], preferred_element_type=jnp.float32
    )
    row_start = lax.axis_index("sp") * own_rows
    own_log = lax.dynamic_slice_in_dim(log_total, row_start, own_rows, 1)
    own_drifts = lax.dynamic_slice_in_dim(drifts, row_start, own_rows, 1)
    pieces = lax.all_gather(own_keys, "sp", axis=1, tiled=True)
    unused, slopes = score_grads(queries, out_grads, pieces[0], pieces[1], own_log, own_drifts)
    query_grads = jnp.einsum("hrs,sd->rhd", slopes, pieces[0], preferred_element_type=jnp.float32)
    summed = split_sums(jnp.stack((key_gradient_rows, value_gradient_rows)), part_cols)
    key_flattened = summed[0].astype(jnp.bfloat16)
    value_flattened = summed[1].astype(jnp.bfloat16)
    weight_part = lax.dot_general(
        block_rows, key_flattened, (((0,), (0,)), ((), ())), preferred_element_type=jnp.float32
    )
    key_weight_grad = gathered_total(weight_part.astype(jnp.bfloat16), "sp").astype(jnp.float32)
    source_upstream = summed_on_arrival(
        (
            times_transposed(key_flattened, key_weight)
            + times_transposed(value_flattened, value_projection_weight)
        ).astype(jnp.bfloat16),
        "tp",
        0,
    )
    source_grad = norm_back(src_scaled, src_inverse, source_gain, source_upstream)
    query_flat = query_grads.astype(jnp.bfloat16).reshape(own_rows, head_count * HEAD_SIZE)
    out_rows = own_rows // lax.axis_size("tp")
    out_start = lax.axis_index("tp") * out_rows
    target_upstream = sent_and_summed(times_transposed(query_flat, query_weight), "tp", 0)
    slice_scaled = lax.dynamic_slice_in_dim(tgt_scaled, out_start, out_rows, 0)
    slice_inverse = lax.dynamic_slice_in_dim(tgt_inverse, out_start, out_rows, 0)
    slice_cotangent = lax.dynamic_slice_in_dim(cotangent, out_start, out_rows, 0)
    target_grad = slice_cotangent.astype(jnp.float32) + norm_back(
        slice_scaled, slice_inverse, target_gain, target_upstream
    )
    return (target_grad, source_grad, key_weight_grad)


def solution(mesh):
    return jax.shard_map(
        on_device,
        mesh=mesh,
        in_specs=(
            P("sp", None),
            P(("sp", "tp"), None),
            P("sp", None),
            P(),
            P(),
            P(None, "tp"),
            P(None, "tp"),
            P(None, "tp"),
            P("tp", None),
        ),
        out_specs=(P(("sp", "tp"), None), P(("sp", "tp"), None), P(None, "tp")),
        check_vma=False,
    )
```

profile of v0, /device:TPU:6, one launch (start us, length us, event | category | flops | bytes accessed | tf_op | source)
XLA Modules:
  0.0 284.7 jit_solution(17369403793125934148)
XLA Ops:
  9.9 1.9 convolution_convert_fusion.1
  13.6 23.2 %all_to_all.20 = bf16[32,8,2048]{2,1,0:T(8,128)(2,1)S(1)} all-to-all(bf16[32,8,2048]{2,1,0:T(8,128)(2,1)S(1)} %broadcast_in_dim.4), channel_id=1, replica_groups=mesh['sp'=16,'tp'=32] {'tp'}, dimensions={0} | all-to-all | bytes 2097152 | tf_op jit(solution)/shard_map/all_to_all | solution.py:20
  37.7 3.3 %collective-permute-start = (bf16[2,256,64]{1,2,0:T(8,128)(2,1)S(1)}, bf16[2,256,64]{1,2,0:T(8,128)(2,1)}, u32[]{:S(2)}, u32[]{:S(2)}) collective-permute-start(bf16[2,256,64]{1,2,0:T(8,128)(2,1)S(1)} %pad_maximum_fusion.2), channel_id=1, source_target_pairs={{0,1},{1,0},{2,3},{3,2},{4,5},{5,4},{6,7},{7,6},{8,9},{9,8},{10,11... | collective-permute-start | bytes 196616 | tf_op jit(solution)/shard_map/ppermute | solution.py:15
  42.9 2.4 collective-permute-start.1
  45.3 5.2 %collective-permute-done.1 = bf16[2,256,128]{1,2,0:T(8,128)(2,1)S(1)} collective-permute-done((bf16[2,256,128]{1,2,0:T(8,128)(2,1)S(1)}, bf16[2,256,128]{1,2,0:T(8,128)(2,1)S(1)}, u32[]{:S(2)}, u32[]{:S(2)}) %collective-permute-start.1) | collective-permute-done | bytes 131104 | tf_op jit(solution)/shard_map/ppermute | solution.py:15
  51.5 38.6 %all-gather.7.cloned.1.call-done = bf16[2048,2,256]{2,0,1:T(8,128)(2,1)} async-done(((bf16[128,2,256]{2,0,1:T(8,128)(2,1)}), bf16[2048,2,256]{2,0,1:T(8,128)(2,1)}) %all-gather.7.cloned.1.call-update) | async-done | bytes 2097168 | tf_op jit(solution)/shard_map/all_gather | solution.py:36
  90.0 1.9 fusion.67
  92.8 28.5 %all_to_all.21 = f32[16,3,2048]{2,1,0:T(4,128)S(1)} all-to-all(f32[16,3,2048]{2,1,0:T(4,128)S(1)} %broadcast_in_dim.5), channel_id=1, replica_groups=mesh['sp'=16,'tp'=32] {'sp'}, dimensions={0} | all-to-all | bytes 786432 | tf_op jit(solution)/shard_map/all_to_all | solution.py:20
  123.9 2.1 collective-permute-start.2
  126.0 6.1 %collective-permute-done.2 = f32[2,256,128]{1,2,0:T(8,128)S(1)} collective-permute-done((f32[2,256,128]{1,2,0:T(8,128)S(1)}, f32[2,256,128]{1,2,0:T(8,128)S(1)}, u32[]{:S(2)}, u32[]{:S(2)}) %collective-permute-start.2) | collective-permute-done | bytes 262176 | tf_op jit(solution)/shard_map/ppermute | solution.py:15
  132.2 1.9 collective-permute-start.3
  137.0 1.4 fusion.9
  138.5 10.5 %all-to-all-start.3 = ((bf16[32,8,2048]{2,1,0:T(8,128)(2,1)}), bf16[32,8,2048]{2,1,0:T(8,128)(2,1)S(1)}, u32[]{:S(2)}, u32[]{:S(2)}) async-start(bf16[32,8,2048]{2,1,0:T(8,128)(2,1)} %fusion.9), calls=%async_computation.3 | async-start | bytes 2097152 | tf_op jit(solution)/shard_map/all_to_all | solution.py:84
  148.9 43.2 %all-gather.5.cloned.1.call-done = bf16[2,4096,256]{1,2,0:T(8,128)(2,1)} async-done(((bf16[2,256,256]{1,2,0:T(8,128)(2,1)}), bf16[2,4096,256]{1,2,0:T(8,128)(2,1)}) %all-gather.5.cloned.1.call-update) | async-done | bytes 4194320 | tf_op jit(solution)/shard_map/all_gather | solution.py:233
  192.2 3.8 %fusion.5 = f32[4096,128,1]{1,0,2:T(8,128)} fusion(bf16[128,256]{1,0:T(8,128)(2,1)S(1)} %convolution_convert_fusion.1, bf16[2,4096,256]{1,2,0:T(8,128)(2,1)} %all-gather.5.cloned.1.call-done, f32[128]{0:T(128)S(1)} %get-tuple-element.24), kind=kOutput, calls=%fused_computation.8 | convolution fusion | flops 268959744 | bytes 4260352 | tf_op jit(solution)/shard_map/rhd,sd->hrs/dot_general | solution.py:145
  195.9 4.4 %fusion.18 = bf16[128,1,256]{2,0,1:T(8,128)(2,1)S(1)} fusion(f32[4096,128,1]{1,0,2:T(8,128)} %fusion.5, bf16[128,256]{1,0:T(8,128)(2,1)S(1)} %copy-done.9, bf16[2,4096,256]{1,2,0:T(8,128)(2,1)} %all-gather.5.cloned.1.call-done, f32[128]{0:T(128)S(1)} %get-tuple-element.23), kind=kOutput, calls=%fused_computation.38 | convolution fusion | flops 539525120 | bytes 6423040 | tf_op jit(solution)/shard_map/hrs,sd->rhd/dot_general | solution.py:235
  200.9 1.7 copy.14
  202.5 6.7 %all-to-all-start.2 = ((f32[32,4,2048]{2,1,0:T(4,128)}), f32[32,4,2048]{2,1,0:T(4,128)}, u32[]{:S(2)}, u32[]{:S(2)}) async-start(f32[32,4,2048]{2,1,0:T(4,128)} %copy.14), calls=%async_computation.2 | async-start | bytes 2097152 | tf_op jit(solution)/shard_map/all_to_all | solution.py:90
  211.7 12.2 %all-to-all-done.2 = f32[32,4,2048]{2,1,0:T(4,128)} async-done(((f32[32,4,2048]{2,1,0:T(4,128)}), f32[32,4,2048]{2,1,0:T(4,128)}, u32[]{:S(2)}, u32[]{:S(2)}) %all-to-all-start.2) | async-done | bytes 1048608 | tf_op jit(solution)/shard_map/all_to_all | solution.py:90
  226.4 1.5 multiply_add_fusion.2
  227.9 40.0 %all-gather.9.cloned.1.call-done = bf16[32768,64]{0,1:T(8,128)(2,1)} async-done(((bf16[2048,64]{0,1:T(8,128)(2,1)}), bf16[32768,64]{0,1:T(8,128)(2,1)}) %all-gather.9.cloned.1.call-update) | async-done | bytes 4194320 | tf_op jit(solution)/shard_map/all_gather | solution.py:74
  267.9 2.7 convert_element_type.93
  270.6 5.0 %copy.15 = f32[8,8,16,2048]{3,2,1,0:T(8,128)S(1)} copy(f32[8,8,16,2048]{3,1,2,0:T(8,128)S(1)} %bitcast.164) | data formatting | bytes 16777216
  275.7 2.5 bitcast_reduce_fusion
  (81 shorter events, 19.6 us)
Async XLA Ops:
  7.2 4.6 %copy-start = (bf16[2048,256]{1,0:T(8,128)(2,1)S(1)}, bf16[2048,256]{1,0:T(8,128)(2,1)}, u32[]{:S(2)}) copy-start(bf16[2048,256]{1,0:T(8,128)(2,1)} %param.14) | copy-start | bytes 3145732
  7.2 4.6 %copy-start.2 = (bf16[128,2048]{1,0:T(8,128)(2,1)S(1)}, bf16[128,2048]{1,0:T(8,128)(2,1)}, u32[]{:S(2)}) copy-start(bf16[128,2048]{1,0:T(8,128)(2,1)} %param.9) | copy-start | bytes 1572868
  7.2 4.6 %copy-start.10 = (f32[2048]{0:T(1024)S(1)}, f32[2048]{0:T(1024)}, u32[]{:S(2)}) copy-start(f32[2048]{0:T(1024)} %param.12) | copy-start | bytes 24580
  7.2 82.8 %all-gather.7.cloned.1.call-start = ((), (), s32[]{:S(2)}) async-start(), calls=%async_computation.5 | async-start | bytes 2228224 | tf_op jit(solution)/shard_map/all_gather | solution.py:36
  9.9 3.1 %copy-start.6 = (bf16[8,2048]{1,0:T(8,128)(2,1)S(1)}, bf16[8,2048]{1,0:T(8,128)(2,1)}, u32[]{:S(2)}) copy-start(bf16[8,2048]{1,0:T(8,128)(2,1)} %param.10) | copy-start | bytes 98308
  9.9 3.4 %copy-start.7 = (f32[2048]{0:T(1024)S(1)}, f32[2048]{0:T(1024)}, u32[]{:S(2)}) copy-start(f32[2048]{0:T(1024)} %param.13) | copy-start | bytes 24580
  12.2 1.1 copy-start.8
  12.2 24.5 %copy-start.4 = (bf16[2048,64]{0,1:T(8,128)(2,1)S(1)}, bf16[2048,64]{0,1:T(8,128)(2,1)}, u32[]{:S(2)}) copy-start(bf16[2048,64]{0,1:T(8,128)(2,1)} %param.16) | copy-start | bytes 786436
  12.9 179.2 %all-gather.5.cloned.1.call-start = ((), (), s32[]{:S(2)}) async-start(), calls=%async_computation.4 | async-start | bytes 4456448 | tf_op jit(solution)/shard_map/all_gather | solution.py:233
  13.4 23.8 %copy-start.5 = (bf16[2048,64]{0,1:T(8,128)(2,1)S(1)}, bf16[2048,64]{0,1:T(8,128)(2,1)}, u32[]{:S(2)}) copy-start(bf16[2048,64]{0,1:T(8,128)(2,1)} %param.15) | copy-start | bytes 786436
  37.7 4.3 %collective-permute-start = (bf16[2,256,64]{1,2,0:T(8,128)(2,1)S(1)}, bf16[2,256,64]{1,2,0:T(8,128)(2,1)}, u32[]{:S(2)}, u32[]{:S(2)}) collective-permute-start(bf16[2,256,64]{1,2,0:T(8,128)(2,1)S(1)} %pad_maximum_fusion.2), channel_id=1, source_target_pairs={{0,1},{1,0},{2,3},{3,2},{4,5},{5,4},{6,7},{7,6},{8,9},{9,8},{10,11... | collective-permute-start | bytes 196616 | tf_op jit(solution)/shard_map/ppermute | solution.py:15
  42.9 7.6 %collective-permute-start.1 = (bf16[2,256,128]{1,2,0:T(8,128)(2,1)S(1)}, bf16[2,256,128]{1,2,0:T(8,128)(2,1)S(1)}, u32[]{:S(2)}, u32[]{:S(2)}) collective-permute-start(bf16[2,256,128]{1,2,0:T(8,128)(2,1)S(1)} %maximum_select_fusion.1), channel_id=1, source_target_pairs={{0,2},{1,3},{2,0},{3,1},{4,6},{5,7},{6,4},{7,5},{8,10},{9,11},{10,... | collective-permute-start | bytes 393224 | tf_op jit(solution)/shard_map/ppermute | solution.py:15
  51.4 40.6 %copy-start.3 = (bf16[2,256,256]{1,2,0:T(8,128)(2,1)S(1)}, bf16[2,256,256]{1,2,0:T(8,128)(2,1)}, u32[]{:S(2)}) copy-start(bf16[2,256,256]{1,2,0:T(8,128)(2,1)} %maximum_select_fusion) | copy-start | bytes 786436
  51.4 216.5 %all-gather.9.cloned.1.call-start = ((), (), s32[]{:S(2)}) async-start(), calls=%async_computation.6 | async-start | bytes 4456448 | tf_op jit(solution)/shard_map/all_gather | solution.py:74
  90.0 2.0 copy-start.1
  123.9 8.3 %collective-permute-start.2 = (f32[2,256,128]{1,2,0:T(8,128)S(1)}, f32[2,256,128]{1,2,0:T(8,128)S(1)}, u32[]{:S(2)}, u32[]{:S(2)}) collective-permute-start(f32[2,256,128]{1,2,0:T(8,128)S(1)} %broadcast_select_fusion), channel_id=1, source_target_pairs={{0,2},{1,3},{2,0},{3,1},{4,6},{5,7},{6,4},{7,5},{8,10},{9,11},{10,... | collective-permute-start | bytes 786440 | tf_op jit(solution)/shard_map/ppermute | solution.py:15
  132.2 3.2 %collective-permute-start.3 = (f32[2,256,64]{1,2,0:T(8,128)S(1)}, f32[2,256,64]{1,2,0:T(8,128)S(1)}, u32[]{:S(2)}, u32[]{:S(2)}) collective-permute-start(f32[2,256,64]{1,2,0:T(8,128)S(1)} %slice_select_fusion), channel_id=1, source_target_pairs={{0,1},{1,0},{2,3},{3,2},{4,5},{5,4},{6,7},{7,6},{8,9},{9,8},{10,11... | collective-permute-start | bytes 393224 | tf_op jit(solution)/shard_map/ppermute | solution.py:15
  138.5 64.1 %all-to-all-start.3 = ((bf16[32,8,2048]{2,1,0:T(8,128)(2,1)}), bf16[32,8,2048]{2,1,0:T(8,128)(2,1)S(1)}, u32[]{:S(2)}, u32[]{:S(2)}) async-start(bf16[32,8,2048]{2,1,0:T(8,128)(2,1)} %fusion.9), calls=%async_computation.3 | async-start | bytes 2097152 | tf_op jit(solution)/shard_map/all_to_all | solution.py:84
  192.2 3.8 %copy-start.9 = (bf16[128,256]{1,0:T(8,128)(2,1)S(1)}, bf16[128,256]{1,0:T(8,128)(2,1)}, u32[]{:S(2)}) copy-start(bf16[128,256]{1,0:T(8,128)(2,1)} %copy-done.8) | copy-start | bytes 196612
  202.5 21.4 %all-to-all-start.2 = ((f32[32,4,2048]{2,1,0:T(4,128)}), f32[32,4,2048]{2,1,0:T(4,128)}, u32[]{:S(2)}, u32[]{:S(2)}) async-start(f32[32,4,2048]{2,1,0:T(4,128)} %copy.14), calls=%async_computation.2 | async-start | bytes 2097152 | tf_op jit(solution)/shard_map/all_to_all | solution.py:90
Sparse Core Ops, SparseCore 0:
  13.0 76.9 all-gather.6
  92.6 99.5 all-gather.4
  194.3 73.5 all-gather.8
where the time goes:
time: 286 us; the launch traced here: 285 us
  waiting for transfers between devices  148 us (52%)
  blocking collectives  51.7 us (18%)
  starting transfers between devices  27 us (9%)
  matrix products  18.7 us (7%)
  other arithmetic  18 us (6%)
  between operations  14.2 us (5%)
  local copies, waits for them, and re-layouts  7.34 us (3%)
    all_to_all x2, blocking collectives, from_everyone(): return lax.all_to_all(copies, axis, split_axis=0, concat_axis=0, tiled=True)  51.7 us
    all_gather x1, waiting for transfers between devices, on_device(): pieces = lax.all_gather(own_keys, 'sp', axis=1, tiled=True)  43.2 us
    all_gather x1, waiting for transfers between devices, gathered_total(): return lax.all_gather(array, axis).astype(jnp.float32).sum(0)  40 us
    all_gather x1, waiting for transfers between devices, side_by_side(): lax.all_gather(both, axis, axis=dim, tiled=True)  38.6 us
    ppermute x4, waiting for transfers between devices, partner_2(): return lax.ppermute(value, axis, pairs)  13.7 us
    all_to_all x1, waiting for transfers between devices, sent_and_summed(): lax.all_to_all(cut_along(array, dim, devices), axis, 0, 0, tiled=True)  12.2 us
    all_to_all x1, starting transfers between devices, summed_on_arrival(): lax.all_to_all(cut_along(array, dim, devices), axis, 0, 0, tiled=True)  10.5 us
    ppermute x4, starting transfers between devices, partner_2(): return lax.ppermute(value, axis, pairs)  9.72 us
  transfers between devices with their start and end apart: 9, of which 8 were waited for; matrix products, arithmetic and copies ran while one was open for 10% of the time, Pallas kernels for 0%

commit v1 on v0

v1 whole, which is shorter than its diff:
```python
import functools
from types import SimpleNamespace

import jax
import jax.numpy as jnp
from jax import lax
from jax.experimental import pallas as pl
from jax.experimental.pallas import tpu as pltpu
from jax.sharding import PartitionSpec as P

MESH = pl.DeviceIdType.MESH
HEAD = 256
EPSILON = 1e-05
SCALE = HEAD**-0.5
f32 = jnp.float32
bf16 = jnp.bfloat16
SUBS = 4


def nt(left, right):
    return lax.dot_general(left, right, (((1,), (1,)), ((), ())), preferred_element_type=f32)


def nn(left, right):
    return jnp.dot(left, right, preferred_element_type=f32)


def norm(rows):
    centred = rows - jnp.mean(rows, axis=-1, keepdims=True)
    inverse = lax.rsqrt(jnp.mean(centred * centred, axis=-1, keepdims=True) + EPSILON)
    return centred * inverse, inverse


def norm_back(scaled, inverse, gain, upstream):
    weighted = upstream * gain
    spread = jnp.mean(weighted * scaled, axis=-1, keepdims=True)
    return inverse * (weighted - jnp.mean(weighted, axis=-1, keepdims=True) - scaled * spread)


def loop(start, stop, body):
    lax.fori_loop(start, stop, lambda i, carry: (body(i), carry)[1], 0)


def kernel(names, Z, T, *refs):
    (target_h, source_h, cot_h, tgain, sgain, wq_h, wk_h, wv_h, wo_h, tgrad, sgrad, wgrad) = refs[:12]
    s = SimpleNamespace(**dict(zip(names, refs[12:])))
    D = wq_h.shape[0]
    TR = target_h.shape[0]
    SR = T * source_h.shape[0]
    C = T // 2
    HALF = D // 2
    PART = wk_h.shape[1]
    G = HEAD // PART
    z = lax.axis_index("sp")
    t = lax.axis_index("tp")
    c = lax.rem(t, 2)
    p = lax.div(t, 2)
    other = t + 1 - 2 * c
    j = lax.rem(t, G)

    def remote(src, dst, send, recv, **where):
        return pltpu.make_async_remote_copy(
            src_ref=src, dst_ref=dst, send_sem=send, recv_sem=recv, device_id=where, device_id_type=MESH
        )

    def zat(k):
        return lax.rem(z + k + Z, Z)

    def chip(k):
        return lax.rem(p + k, C)

    def same(k):
        return 2 * chip(k) + c

    def mate(k):
        return t - j + lax.rem(j + k, G)

    row0 = pl.multiple_of(p * (TR // C), TR // C)
    loads = [
        pltpu.make_async_copy(a, b, s.in_sem.at[i])
        for i, (a, b) in enumerate(
            (
                (source_h, s.src),
                (target_h, s.tgt),
                (wq_h, s.wq),
                (cot_h, s.cot),
                (wo_h, s.wo),
                (wk_h, s.wk),
                (wv_h, s.wv),
                (target_h.at[pl.ds(row0, TR // C), :], s.t8),
                (cot_h.at[pl.ds(row0, TR // C), :], s.c8),
            )
        )
    ]
    for one in loads:
        one.start()

    barrier = pltpu.get_barrier_semaphore()

    def greet(**where):
        pl.semaphore_signal(barrier, inc=1, device_id=where, device_id_type=MESH)

    loop(1, Z, lambda k: greet(sp=zat(k)))
    loop(1, C, lambda k: greet(tp=same(k)))
    greet(tp=other)
    greet(tp=mate(2) + 1 - 2 * c)

    loads[0].wait()
    scaled, inverse = norm(s.src[...].astype(f32))
    s.src_scaled[...] = scaled
    s.src_inv[...] = jnp.broadcast_to(inverse, s.src_inv.shape)
    s.g[t] = (scaled * sgain[...]).astype(bf16)
    loads[1].wait()

    def norm_target(i):
        rows = pl.ds(pl.multiple_of(i * 32, 32), 32)
        values, _ = norm(s.tgt[rows, :].astype(f32))
        s.tn[rows, :] = (values * tgain[...]).astype(bf16)

    loop(0, TR // 32, norm_target)
    own = pl.ds(pl.multiple_of(z * TR, TR), TR)
    loads[2].wait()
    s.qd[own, 0:HEAD] = nn(s.tn[...], s.wq[...]).astype(bf16)
    loads[3].wait()
    loads[4].wait()
    s.qd[own, HEAD : 2 * HEAD] = nt(s.cot[...], s.wo[...]).astype(bf16)
    pl.semaphore_wait(barrier, (Z - 1) + (C - 1) + 2)

    def source_copy(k):
        return remote(s.g.at[t], s.g.at[t], s.src_send.at[k], s.src_recv.at[t], tp=same(k))

    loop(1, C, lambda k: source_copy(k).start())

    def forward_copy(k):
        row = s.g.at[same(k)]
        return remote(row, row, s.fwd_send.at[k], s.src_recv.at[same(k)], tp=other)

    forward_copy(0).start()
    rows_sub = TR // SUBS

    def ring_copy(block, sub, way, step):
        rows = s.qd.at[pl.ds(pl.multiple_of(block * TR + sub * rows_sub, rows_sub), rows_sub), :]
        return remote(
            rows, rows, s.ring_send.at[way, step, sub], s.ring_recv.at[way, step, sub],
            sp=zat(1 if way == 0 else -1),
        )

    H = Z // 2

    def reach(way, step):
        if step < H:
            return 0, SUBS
        return (0, SUBS // 2) if way == 0 else (SUBS // 2, SUBS)

    for way in (0, 1):
        loop(*reach(way, 1), lambda sub: ring_copy(z, sub, way, 1).start())

    def ring(step):
        for way in (0, 1):
            block = zat(-step if way == 0 else step)
            lo, hi = reach(way, step)
            flo, fhi = reach(way, step + 1) if step < H else (0, 0)

            def arrive(sub, on):
                ring_copy(block, sub, way, step).wait_recv()
                if on:
                    ring_copy(block, sub, way, step + 1).start()

            if (flo, fhi) == (lo, hi):
                loop(lo, hi, lambda sub: arrive(sub, True))
            else:
                for sub in range(lo, hi):
                    arrive(sub, flo <= sub < fhi)

    loads[5].wait()
    loads[6].wait()

    def join_weights(i):
        rows = pl.ds(pl.multiple_of(i * 256, 256), 256)
        both = jnp.concatenate((s.wk[rows, :].astype(f32), s.wv[rows, :].astype(f32)), axis=1)
        s.wkv[rows, :] = both.astype(bf16)

    loop(0, D // 256, join_weights)

    ring(1)

    def pass_on(k):
        source_copy_from(k).wait_recv()
        forward_copy(k).start()

    def source_copy_from(k):
        row = s.g.at[same(k)]
        return remote(row, row, s.src_send.at[k], s.src_recv.at[same(k)], tp=other)

    loop(1, C, pass_on)
    ring(2)

    def from_other(k):
        at = 2 * chip(k) + 1 - c
        remote(s.g.at[at], s.g.at[at], s.src_send.at[k], s.src_recv.at[at], tp=other).wait_recv()

    loop(0, C, from_other)

    def stack_rows(q):
        both = jnp.concatenate((s.g[2 * q].astype(f32), s.g[2 * q + 1].astype(f32)), axis=0)
        s.rows[pl.ds(pl.multiple_of(q * 16, 16), 16), :] = both.astype(bf16)

    loop(0, C, stack_rows)
    s.kvp[j] = nn(s.rows[...], s.wkv[...]).astype(bf16)

    def join_copy(k):
        return remote(s.kvp.at[j], s.kvp.at[j], s.join_send.at[k], s.join_recv.at[j], tp=mate(k))

    for k in range(1, G):
        join_copy(k).start()
    ring(3)
    for k in range(1, G):
        at = lax.rem(j + k, G)
        remote(s.kvp.at[at], s.kvp.at[at], s.join_send.at[k], s.join_recv.at[at], tp=other).wait_recv()
    parts = [s.kvp[i].astype(f32) for i in range(G)]
    keys = jnp.concatenate([a[:, :PART] for a in parts], axis=1)
    s.keys[...] = keys.astype(bf16)
    s.keys_t[...] = keys.T.astype(bf16)
    s.values[...] = jnp.concatenate([a[:, PART:] for a in parts], axis=1).astype(bf16)

    def block_of(k):
        return zat(lax.div(k + 1, 2) * (2 * lax.rem(k, 2) - 1))

    def stat_copy(k):
        b = block_of(k)
        return remote(s.stat.at[b], s.got.at[z], s.stat_send.at[k], s.stat_recv.at[z], sp=b)

    def scores(k):
        b = block_of(k)
        rows = pl.ds(pl.multiple_of(b * TR, TR), TR)
        scores_t = nt(s.keys[...], s.qd[rows, 0:HEAD]) * SCALE
        products_t = nt(s.values[...], s.qd[rows, HEAD : 2 * HEAD])
        highest = jnp.max(scores_t, axis=0, keepdims=True)
        weights = jnp.exp(scores_t - highest)
        s.e[b] = weights
        s.p[b] = products_t
        s.stat[b, 0:1, :] = highest
        s.stat[b, 1:2, :] = jnp.sum(weights, axis=0, keepdims=True)
        s.stat[b, 2:3, :] = jnp.sum(weights * products_t, axis=0, keepdims=True)
        s.stat[b, 3:4, :] = highest

    def scores_sent(k):
        scores(k)
        stat_copy(k).start()

    ring(4)
    scores(0)
    s.got[z] = s.stat[z]
    loop(1, 3, scores_sent)
    ring(5)
    loop(3, 7, scores_sent)
    ring(6)
    loop(7, 11, scores_sent)
    ring(7)
    loop(11, 15, scores_sent)
    ring(8)
    loop(15, 16, scores_sent)

    def stat_wait(k):
        at = block_of(k)
        remote(s.stat.at[at], s.got.at[at], s.stat_send.at[k], s.stat_recv.at[at], sp=at).wait_recv()

    loop(1, Z, stat_wait)
    top = lax.fori_loop(
        1, Z, lambda i, a: jnp.maximum(a, s.got[i, 0:1, :]), s.got[0, 0:1, :]
    )

    def add_stats(i, sums):
        factor = jnp.exp(s.got[i, 0:1, :] - top)
        return sums[0] + s.got[i, 1:2, :] * factor, sums[1] + s.got[i, 2:3, :] * factor

    total, weighted = lax.fori_loop(0, Z, add_stats, (jnp.zeros_like(top), jnp.zeros_like(top)))
    s.fin[z, 0:1, :] = top + jnp.log(total)
    s.fin[z, 1:2, :] = weighted / total

    def fin_copy(k):
        return remote(s.fin.at[z], s.fin.at[z], s.fin_send.at[k], s.fin_recv.at[z], sp=block_of(k))

    loop(1, Z, lambda k: fin_copy(k).start())

    def fin_wait(k):
        at = block_of(k)
        remote(s.fin.at[at], s.fin.at[at], s.fin_send.at[k], s.fin_recv.at[at], sp=at).wait_recv()

    loop(1, Z, fin_wait)

    def slopes(b):
        cols = pl.ds(pl.multiple_of(b * TR, TR), TR)
        weights = s.e[b] * jnp.exp(s.stat[b, 0:1, :] - s.fin[b, 0:1, :])
        s.att[:, cols] = weights.astype(bf16)
        s.slo[:, cols] = (weights * (s.p[b] - s.fin[b, 1:2, :]) * SCALE).astype(bf16)

    loop(0, Z, slopes)
    s.dq[...] = nn(s.keys_t[...], s.slo[...])

    hd = HEAD // 2

    def hops(way, sub):
        return H if way == sub else H - 1

    def dq_copy(way, step, sub):
        return remote(
            s.dq_out.at[way, step, sub], s.dq_in.at[way, step, sub],
            s.dq_send.at[way, step, sub], s.dq_recv.at[way, step, sub],
            sp=zat(-1 if way == 0 else 1),
        )

    def dq_ring(step):
        for sub in (0, 1):
            for way in (0, 1):
                if step > hops(way, sub):
                    continue
                far = hops(way, sub) + 1 - step
                b = zat(-far if way == 0 else far)
                mine = s.dq[sub * hd : (sub + 1) * hd, pl.ds(pl.multiple_of(b * TR, TR), TR)]
                if step > 1:
                    dq_copy(way, step - 1, sub).wait_recv()
                    mine = mine + s.dq_in[way, step - 1, sub].astype(f32)
                s.dq_out[way, step, sub] = mine.astype(bf16)
                dq_copy(way, step, sub).start()

    dq_ring(1)

    dk = nn(s.slo[...], s.qd[:, 0:HEAD])
    dv = nn(s.att[...], s.qd[:, HEAD : 2 * HEAD])
    for i in range(G):
        cut = slice(i * PART, (i + 1) * PART)
        s.dkv[i] = jnp.concatenate((dk[:, cut], dv[:, cut]), axis=1)
    for k in range(1, G):
        s.dkv_out[k] = s.dkv[lax.rem(j + k, G)].astype(bf16)

    def dkv_copy(k):
        return remote(s.dkv_out.at[k], s.dkv_in.at[k], s.dkv_send.at[k], s.dkv_recv.at[k], tp=mate(k))

    for k in range(1, G):
        dkv_copy(k).start()
    dq_ring(2)
    flat = s.dkv[j]
    for k in range(1, G):
        dkv_copy(k).wait_recv()
        flat = flat + s.dkv_in[k].astype(f32)
    s.flat[...] = flat.astype(bf16)

    part_t = nn(flat.T[:PART, :].astype(bf16), s.rows[...])
    CW = D // Z
    for i in range(Z):
        s.wp[i] = part_t[:, i * CW : (i + 1) * CW].astype(bf16)
    s.wr[z] = s.wp[z]

    def wr_copy(k):
        return remote(s.wp.at[block_of(k)], s.wr.at[z], s.wr_send.at[k], s.wr_recv.at[z], sp=block_of(k))

    loop(1, Z, lambda k: wr_copy(Z - k).start())

    s.su[...] = nt(s.flat[...], s.wkv[...])

    def for_other(q):
        s.ss[q] = s.su[pl.ds(pl.multiple_of(q * 16 + 8 * (1 - c), 8), 8), :].astype(bf16)

    loop(0, C, for_other)
    su_pair = remote(s.ss, s.sr, s.pair_send.at[0], s.pair_recv.at[0], tp=other)
    su_pair.start()
    dq_ring(3)
    su_pair.wait_recv()

    def sw_copy(k):
        return remote(s.sv.at[chip(k)], s.sw.at[p], s.sw_send.at[k], s.sw_recv.at[p], tp=same(k))

    def both_cores(k):
        q = chip(k)
        mine = s.su[pl.ds(pl.multiple_of(q * 16 + 8 * c, 8), 8), :]
        return (mine + s.sr[q].astype(f32)).astype(bf16)

    s.sw[p] = both_cores(0)

    def sw_start(k):
        s.sv[chip(k)] = both_cores(k)
        sw_copy(k).start()

    loop(1, C, sw_start)
    dq_ring(4)
    dq_ring(5)

    def wr_wait(k):
        at = block_of(k)
        remote(s.wp.at[at], s.wr.at[at], s.wr_send.at[k], s.wr_recv.at[at], sp=at).wait_recv()

    loop(1, Z, wr_wait)
    s.wf[z] = lax.fori_loop(
        1, Z, lambda i, a: a + s.wr[i].astype(f32), s.wr[0].astype(f32)
    ).astype(bf16)

    def wf_copy(k):
        return remote(s.wf.at[z], s.wf.at[z], s.wf_send.at[k], s.wf_recv.at[z], sp=block_of(k))

    loop(1, Z, lambda k: wf_copy(Z - k).start())
    dq_ring(6)

    def sw_wait(k):
        at = chip(k)
        remote(s.sv.at[at], s.sw.at[at], s.sw_send.at[k], s.sw_recv.at[at], tp=other).wait_recv()

    loop(1, C, sw_wait)
    s.su8[...] = s.sw[0].astype(f32)

    def add_sw(i):
        s.su8[...] += s.sw[i].astype(f32)

    loop(1, C, add_sw)
    sgrad[...] = norm_back(s.src_scaled[...], s.src_inv[:, 0:1], sgain[...], s.su8[...])
    dq_ring(7)
    dq_ring(8)
    halves = []
    for sub in (0, 1):
        mine = s.dq[sub * hd : (sub + 1) * hd, own]
        for way in (0, 1):
            last = hops(way, sub)
            dq_copy(way, last, sub).wait_recv()
            mine = mine + s.dq_in[way, last, sub].astype(f32)
        halves.append(mine)
    query_flat = jnp.concatenate(halves, axis=0).T.astype(bf16)

    TB = TR // C

    def half_cols(h):
        return s.wq[pl.ds(pl.multiple_of(h * HALF, HALF), HALF), :]

    s.tsend[...] = nt(query_flat, half_cols(1 - c)).reshape(C, TB, HALF).astype(bf16)
    tu_pair = remote(s.tsend, s.trecv, s.pair_send.at[1], s.pair_recv.at[1], tp=other)
    tu_pair.start()
    s.tmine[...] = nt(query_flat, half_cols(c)).reshape(C, TB, HALF)
    tu_pair.wait_recv()

    def tw_copy(k):
        return remote(s.tv.at[chip(k)], s.tw.at[p], s.tw_send.at[k], s.tw_recv.at[p], tp=same(k))

    def tboth(k):
        q = chip(k)
        return (s.tmine[q] + s.trecv[q].astype(f32)).astype(bf16)

    s.tw[p] = tboth(0)

    def tw_start(k):
        s.tv[chip(k)] = tboth(k)
        tw_copy(k).start()

    loop(1, C, tw_start)

    def wf_wait(k):
        at = block_of(k)
        remote(s.wf.at[at], s.wf.at[at], s.wf_send.at[k], s.wf_recv.at[at], sp=at).wait_recv()

    loop(1, Z, wf_wait)

    def put_weight(i):
        wgrad[pl.ds(pl.multiple_of(i * CW, CW), CW), :] = s.wf[i].astype(f32).T

    loop(0, Z, put_weight)

    def tw_wait(k):
        at = chip(k)
        remote(s.tv.at[at], s.tw.at[at], s.tw_send.at[k], s.tw_recv.at[at], tp=other).wait_recv()

    loop(1, C, tw_wait)
    s.tu8[...] = s.tw[0].astype(f32)

    def add_tw(i):
        s.tu8[...] += s.tw[i].astype(f32)

    loop(1, C, add_tw)
    TO = TB // 2
    lower, upper = s.tu8[0:TO, :], s.tu8[TO:TB, :]
    mine = jnp.where(c == 0, lower, upper)
    s.tx_out[...] = jnp.where(c == 0, upper, lower)
    last_pair = remote(s.tx_out, s.tx_in, s.pair_send.at[2], s.pair_recv.at[2], tp=other)
    last_pair.start()
    loads[7].wait()
    loads[8].wait()
    scaled, inverse = norm(s.t8[...].astype(f32))
    cot = s.c8[...].astype(f32)
    scaled = jnp.where(c == 0, scaled[0:TO], scaled[TO:TB])
    inverse = jnp.where(c == 0, inverse[0:TO], inverse[TO:TB])
    cot = jnp.where(c == 0, cot[0:TO], cot[TO:TB])
    last_pair.wait_recv()
    theirs = s.tx_in[...]
    upstream = jnp.concatenate(
        (jnp.where(c == 0, mine, theirs), jnp.where(c == 0, theirs, mine)), axis=1
    )
    tgrad[...] = cot + norm_back(scaled, inverse, tgain[...], upstream)

    loop(1, C, lambda k: source_copy(k).wait_send())
    loop(0, C, lambda k: forward_copy(k).wait_send())
    for way in (0, 1):
        for step in range(1, H + 1):
            block = zat(-(step - 1) if way == 0 else step - 1)
            loop(*reach(way, step), lambda sub: ring_copy(block, sub, way, step).wait_send())
    for k in range(1, G):
        join_copy(k).wait_send()
        dkv_copy(k).wait_send()

    def line_sends(k):
        stat_copy(k).wait_send()
        fin_copy(k).wait_send()
        wr_copy(k).wait_send()
        wf_copy(k).wait_send()

    loop(1, Z, line_sends)
    for way in (0, 1):
        for sub in (0, 1):
            for step in range(1, hops(way, sub) + 1):
                dq_copy(way, step, sub).wait_send()

    def plane_sends(k):
        sw_copy(k).wait_send()
        tw_copy(k).wait_send()

    loop(1, C, plane_sends)
    su_pair.wait_send()
    tu_pair.wait_send()
    last_pair.wait_send()


def solution(mesh):
    Z, T = mesh.shape["sp"], mesh.shape["tp"]

    def on_device(target, source, cotangent, target_gain, source_gain, wq, wk, wv, wo):
        TR, D = target.shape
        SB = source.shape[0]
        SR = SB * T
        C = T // 2
        PART = wk.shape[1]
        G = HEAD // PART
        H = Z // 2
        TB = TR // C
        CW = D // Z
        V = pltpu.VMEM
        dma = pltpu.SemaphoreType.DMA
        scratch = dict(
            src=V((SB, D), bf16), tgt=V((TR, D), bf16), cot=V((TR, D), bf16),
            wq=V((D, HEAD), bf16), wk=V((D, PART), bf16), wv=V((D, PART), bf16), wo=V((HEAD, D), bf16),
            t8=V((TB, D), bf16), c8=V((TB, D), bf16),
            src_scaled=V((SB, D), f32), src_inv=V((SB, 128), f32),
            g=V((T, SB, D), bf16), tn=V((TR, D), bf16), qd=V((Z * TR, 2 * HEAD), bf16),
            wkv=V((D, 2 * PART), bf16), rows=V((SR, D), bf16), kvp=V((G, SR, 2 * PART), bf16),
            keys=V((SR, HEAD), bf16), keys_t=V((HEAD, SR), bf16), values=V((SR, HEAD), bf16),
            e=V((Z, SR, TR), f32), p=V((Z, SR, TR), f32),
            stat=V((Z, 4, TR), f32), got=V((Z, 4, TR), f32), fin=V((Z, 2, TR), f32),
            att=V((SR, Z * TR), bf16), slo=V((SR, Z * TR), bf16), dq=V((HEAD, Z * TR), f32),
            dq_out=V((2, H + 1, 2, HEAD // 2, TR), bf16), dq_in=V((2, H + 1, 2, HEAD // 2, TR), bf16),
            dkv=V((G, SR, 2 * PART), f32), dkv_out=V((G, SR, 2 * PART), bf16), dkv_in=V((G, SR, 2 * PART), bf16),
            flat=V((SR, 2 * PART), bf16),
            wp=V((Z, PART, CW), bf16), wr=V((Z, PART, CW), bf16), wf=V((Z, PART, CW), bf16),
            su=V((SR, D), f32), ss=V((C, SB, D), bf16), sr=V((C, SB, D), bf16),
            sv=V((C, SB, D), bf16), sw=V((C, SB, D), bf16), su8=V((SB, D), f32),
            tsend=V((C, TB, D // 2), bf16), trecv=V((C, TB, D // 2), bf16), tmine=V((C, TB, D // 2), f32),
            tv=V((C, TB, D // 2), bf16), tw=V((C, TB, D // 2), bf16), tu8=V((TB, D // 2), f32),
            tx_out=V((TB // 2, D // 2), f32), tx_in=V((TB // 2, D // 2), f32),
            in_sem=dma((9,)), src_send=dma((C,)), fwd_send=dma((C,)), src_recv=dma((T,)),
            ring_send=dma((2, H + 1, SUBS)), ring_recv=dma((2, H + 1, SUBS)),
            join_send=dma((G,)), join_recv=dma((G,)), dkv_send=dma((G,)), dkv_recv=dma((G,)),
            stat_send=dma((Z,)), stat_recv=dma((Z,)), fin_send=dma((Z,)), fin_recv=dma((Z,)),
            wr_send=dma((Z,)), wr_recv=dma((Z,)), wf_send=dma((Z,)), wf_recv=dma((Z,)),
            dq_send=dma((2, H + 1, 2)), dq_recv=dma((2, H + 1, 2)),
            sw_send=dma((C,)), sw_recv=dma((C,)), tw_send=dma((C,)), tw_recv=dma((C,)),
            pair_send=dma((3,)), pair_recv=dma((3,)),
        )
        vmem = pl.BlockSpec(memory_space=pltpu.VMEM)
        any_ = pl.BlockSpec(memory_space=pl.ANY)
        return pl.pallas_call(
            functools.partial(kernel, tuple(scratch), Z, T),
            out_shape=(
                jax.ShapeDtypeStruct((TR // T, D), f32),
                jax.ShapeDtypeStruct((SB, D), f32),
                jax.ShapeDtypeStruct((D, PART), f32),
            ),
            in_specs=[any_, any_, any_, vmem, vmem, any_, any_, any_, any_],
            out_specs=(vmem, vmem, vmem),
            scratch_shapes=list(scratch.values()),
            compiler_params=pltpu.CompilerParams(
                collective_id=0, has_side_effects=True, vmem_limit_bytes=62 * 1024 * 1024
            ),
            name="backward",
        )(target, source, cotangent, target_gain.reshape(1, D), source_gain.reshape(1, D), wq, wk, wv, wo)

    return jax.shard_map(
        on_device,
        mesh=mesh,
        in_specs=(
            P("sp", None), P(("sp", "tp"), None), P("sp", None), P(), P(),
            P(None, "tp"), P(None, "tp"), P(None, "tp"), P("tp", None),
        ),
        out_specs=(P(("sp", "tp"), None), P(("sp", "tp"), None), P(None, "tp")),
        check_vma=False,
    )
```

time: 286 us -> 135 us (0.47)
  the two profiles are of different devices: /device:TPU:6 before, /device:TPU:1 now
where the time goes in v1:
time: 135 us
  Pallas kernels  127 us (94%)
  local copies, waits for them, and re-layouts  6.84 us (5%)
    pallas_call x1, Pallas kernels, on_device(): pl.pallas_call(functools.partial(kernel, tuple(scratch), Z, T), out_shape...  127 us
    unnamed x10, local copies, waits for them, and re-layouts  4.5 us

profile of v1, /device:TPU:1, one launch (start us, length us, event | category | flops | bytes accessed | tf_op | source)
XLA Modules:
  0.0 134.8 jit_solution(10333335999708763895)
XLA Ops:
  0.6 0.0 copy-start
  0.6 2.0 %copy.12.refs_6_ = bf16[2048,64]{1,0:T(8,128)(2,1)} copy(bf16[2048,64]{0,1:T(8,128)(2,1)} %param.15) | data formatting | bytes 524288 | tf_op args[6]
  2.6 0.0 copy-done
  2.6 1.0 copy.13.refs_7_
  3.7 127.3 %backward.1 = (f32[4,2048]{1,0:T(4,128)}, f32[8,2048]{1,0:T(8,128)}, f32[2048,64]{1,0:T(8,128)}) custom-call(bf16[128,2048]{1,0:T(8,128)(2,1)} %refs_0_.1, bf16[8,2048]{1,0:T(8,128)(2,1)} %refs_1_.1, bf16[128,2048]{1,0:T(8,128)(2,1)} %refs_2_.1, f32[1,2048]{1,0:T(1,128)} %bitcast.2, f32[1,2048]{1,0:T(1,128)} %bitcast.3, bf16[2048,256]{1,0:T(8,128)(2,1)} %refs_5_.1, ...), custom_call_target="tpu_custom_call" | custom-call | tf_op jit(solution)/shard_map/backward/pallas_call | solution.py:574
  131.0 0.0 copy-start.2
  131.0 2.3 %copy.14 = f32[2048,64]{0,1:T(8,128)} copy(f32[2048,64]{1,0:T(8,128)} %get-tuple-element.5) | data formatting | bytes 1048576 | tf_op jit(solution)/shard_map/backward/pallas_call | solution.py:574
  133.3 0.0 copy-done.2
  133.3 0.0 copy-start.1
  133.3 0.6 copy.17
  133.9 0.2 copy-done.1
  134.2 0.6 copy.18
Async XLA Ops:
  0.6 2.0 %copy-start = (bf16[2048,64]{0,1:T(8,128)(2,1)S(1)}, bf16[2048,64]{0,1:T(8,128)(2,1)}, u32[]{:S(2)}) copy-start(bf16[2048,64]{0,1:T(8,128)(2,1)} %param.16) | copy-start | bytes 786436
  131.0 2.4 %copy-start.2 = (f32[4,2048]{1,0:T(4,128)S(1)}, f32[4,2048]{1,0:T(4,128)}, u32[]{:S(2)}) copy-start(f32[4,2048]{1,0:T(4,128)} %get-tuple-element.9) | copy-start | bytes 98308
  133.3 0.9 copy-start.1

commit v2 on v1

--- a/solution.py
+++ b/solution.py
@@ -49,7 +49,7 @@
     SR = T * source_h.shape[0]
     C = T // 2
     HALF = D // 2
-    PART = wk_h.shape[1]
+    PART = wk_h.shape[0]
     G = HEAD // PART
     z = lax.axis_index("sp")
     t = lax.axis_index("tp")
@@ -85,8 +85,8 @@
                 (wq_h, s.wq),
                 (cot_h, s.cot),
                 (wo_h, s.wo),
-                (wk_h, s.wk),
-                (wv_h, s.wv),
+                (wk_h, s.wkv.at[0:PART, :]),
+                (wv_h, s.wkv.at[PART : 2 * PART, :]),
                 (target_h.at[pl.ds(row0, TR // C), :], s.t8),
                 (cot_h.at[pl.ds(row0, TR // C), :], s.c8),
             )
@@ -155,32 +155,39 @@
     for way in (0, 1):
         loop(*reach(way, 1), lambda sub: ring_copy(z, sub, way, 1).start())
 
-    def ring(step):
-        for way in (0, 1):
+    def ring(step, first=-1):
+        def arrive(way, sub, on):
             block = zat(-step if way == 0 else step)
-            lo, hi = reach(way, step)
-            flo, fhi = reach(way, step + 1) if step < H else (0, 0)
-
-            def arrive(sub, on):
-                ring_copy(block, sub, way, step).wait_recv()
-                if on:
-                    ring_copy(block, sub, way, step + 1).start()
-
-            if (flo, fhi) == (lo, hi):
-                loop(lo, hi, lambda sub: arrive(sub, True))
-            else:
-                for sub in range(lo, hi):
-                    arrive(sub, flo <= sub < fhi)
+            ring_copy(block, sub, way, step).wait_recv()
+            if on:
+                ring_copy(block, sub, way, step + 1).start()
+
+        def both(lo, hi, on):
+            def at(sub):
+                arrive(0, sub, on[0])
+                arrive(1, sub, on[1])
+                if first >= 0:
+                    scores_sent(first + sub)
+
+            loop(lo, hi, at)
+
+        if step < H - 1:
+            both(0, SUBS, (True, True))
+        elif step == H - 1:
+            both(0, SUBS // 2, (True, False))
+            both(SUBS // 2, SUBS, (False, True))
+        else:
+
+            def last(sub):
+                arrive(0, sub, False)
+                arrive(1, SUBS // 2 + sub, False)
+                if first >= 0:
+                    scores_sent(first + sub)
+
+            loop(0, SUBS // 2, last)
 
     loads[5].wait()
     loads[6].wait()
-
-    def join_weights(i):
-        rows = pl.ds(pl.multiple_of(i * 256, 256), 256)
-        both = jnp.concatenate((s.wk[rows, :].astype(f32), s.wv[rows, :].astype(f32)), axis=1)
-        s.wkv[rows, :] = both.astype(bf16)
-
-    loop(0, D // 256, join_weights)
 
     ring(1)
 
@@ -206,7 +213,7 @@
         s.rows[pl.ds(pl.multiple_of(q * 16, 16), 16), :] = both.astype(bf16)
 
     loop(0, C, stack_rows)
-    s.kvp[j] = nn(s.rows[...], s.wkv[...]).astype(bf16)
+    s.kvp[j] = nt(s.rows[...], s.wkv[...]).astype(bf16)
 
     def join_copy(k):
         return remote(s.kvp.at[j], s.kvp.at[j], s.join_send.at[k], s.join_recv.at[j], tp=mate(k))
@@ -214,6 +221,7 @@
     for k in range(1, G):
         join_copy(k).start()
     ring(3)
+    ring(4)
     for k in range(1, G):
         at = lax.rem(j + k, G)
         remote(s.kvp.at[at], s.kvp.at[at], s.join_send.at[k], s.join_recv.at[at], tp=other).wait_recv()
@@ -228,7 +236,7 @@
 
     def stat_copy(k):
         b = block_of(k)
-        return remote(s.stat.at[b], s.got.at[z], s.stat_send.at[k], s.stat_recv.at[z], sp=b)
+        return remote(s.stat.at[b], s.got.at[z], s.stat_send.at[k], s.stat_recv.at[z], sp=lax.rem(b + H, Z))
 
     def scores(k):
         b = block_of(k)
@@ -248,18 +256,14 @@
         scores(k)
         stat_copy(k).start()
 
-    ring(4)
-    scores(0)
-    s.got[z] = s.stat[z]
-    loop(1, 3, scores_sent)
-    ring(5)
-    loop(3, 7, scores_sent)
-    ring(6)
-    loop(7, 11, scores_sent)
-    ring(7)
-    loop(11, 15, scores_sent)
-    ring(8)
-    loop(15, 16, scores_sent)
+    ring(5, 0)
+    ring(6, 4)
+    ring(7, 8)
+    ring(8, 12)
+    loop(14, 15, scores_sent)
+    scores(15)
+    far = zat(H)
+    s.got[z] = s.stat[far]
 
     def stat_wait(k):
         at = block_of(k)
@@ -275,16 +279,16 @@
         return sums[0] + s.got[i, 1:2, :] * factor, sums[1] + s.got[i, 2:3, :] * factor
 
     total, weighted = lax.fori_loop(0, Z, add_stats, (jnp.zeros_like(top), jnp.zeros_like(top)))
-    s.fin[z, 0:1, :] = top + jnp.log(total)
-    s.fin[z, 1:2, :] = weighted / total
+    s.fin[far, 0:1, :] = top + jnp.log(total)
+    s.fin[far, 1:2, :] = weighted / total
 
     def fin_copy(k):
-        return remote(s.fin.at[z], s.fin.at[z], s.fin_send.at[k], s.fin_recv.at[z], sp=block_of(k))
-
-    loop(1, Z, lambda k: fin_copy(k).start())
+        return remote(s.fin.at[far], s.fin.at[far], s.fin_send.at[k], s.fin_recv.at[far], sp=block_of(k))
+
+    loop(1, Z, lambda k: fin_copy(Z - k).start())
 
     def fin_wait(k):
-        at = block_of(k)
+        at = block_of(k - 1)
         remote(s.fin.at[at], s.fin.at[at], s.fin_send.at[k], s.fin_recv.at[at], sp=at).wait_recv()
 
     loop(1, Z, fin_wait)
@@ -340,6 +344,7 @@
     for k in range(1, G):
         dkv_copy(k).start()
     dq_ring(2)
+    dq_ring(3)
     flat = s.dkv[j]
     for k in range(1, G):
         dkv_copy(k).wait_recv()
@@ -350,14 +355,59 @@
     CW = D // Z
     for i in range(Z):
         s.wp[i] = part_t[:, i * CW : (i + 1) * CW].astype(bf16)
-    s.wr[z] = s.wp[z]
-
-    def wr_copy(k):
-        return remote(s.wp.at[block_of(k)], s.wr.at[z], s.wr_send.at[k], s.wr_recv.at[z], sp=block_of(k))
-
-    loop(1, Z, lambda k: wr_copy(Z - k).start())
-
-    s.su[...] = nt(s.flat[...], s.wkv[...])
+    R = H // 2
+
+    def sign(way, k):
+        return zat(k if way == 1 else -k)
+
+    def w_copy(way, k):
+        hop = k % R or R
+        src = s.w_rel.at[way] if k == R else s.wp.at[sign(way, k)]
+        return remote(src, s.w_in.at[way, k], s.w_send.at[way, k], s.w_recv.at[way, k], sp=sign(way, hop))
+
+    top_hop = (2 * R, 2 * R - 1)
+    for way in (0, 1):
+        for k in range(top_hop[way], 0, -1):
+            if k != R:
+                w_copy(way, k).start()
+
+    def w_relay():
+        for way in (0, 1):
+            total = s.wp[sign(way, R)].astype(f32)
+            for k in range(R + 1, top_hop[way] + 1):
+                w_copy(way, k).wait_recv()
+                total = total + s.w_in[way, k].astype(f32)
+            s.w_rel[way] = total.astype(bf16)
+            w_copy(way, R).start()
+
+    def f_copy(way, k, relay):
+        block = sign(1 - way, R) if relay else z
+        hop = k - R if relay else k
+        return remote(s.wf.at[block], s.wf.at[block], s.f_send.at[way, k], s.f_recv.at[block], sp=sign(way, hop))
+
+    def w_owner():
+        total = s.wp[z].astype(f32)
+        for way in (0, 1):
+            for k in range(1, R + 1):
+                w_copy(way, k).wait_recv()
+                total = total + s.w_in[way, k].astype(f32)
+        s.wf[z] = total.astype(bf16)
+        for way in (0, 1):
+            for k in range(R, 0, -1):
+                f_copy(way, k, False).start()
+
+    def f_wait(k):
+        at = block_of(k)
+        remote(s.wf.at[at], s.wf.at[at], s.f_send.at[0, k % 2], s.f_recv.at[at], sp=at).wait_recv()
+
+    def f_relay():
+        for way in (0, 1):
+            f_wait(2 * R - 1 if way == 0 else 2 * R)
+            for k in range(top_hop[way], R, -1):
+                f_copy(way, k, True).start()
+
+    dq_ring(4)
+    s.su[...] = nn(s.flat[...], s.wkv[...])
 
     def for_other(q):
         s.ss[q] = s.su[pl.ds(pl.multiple_of(q * 16 + 8 * (1 - c), 8), 8), :].astype(bf16)
@@ -365,7 +415,7 @@
     loop(0, C, for_other)
     su_pair = remote(s.ss, s.sr, s.pair_send.at[0], s.pair_recv.at[0], tp=other)
     su_pair.start()
-    dq_ring(3)
+    dq_ring(5)
     su_pair.wait_recv()
 
     def sw_copy(k):
@@ -383,38 +433,11 @@
         sw_copy(k).start()
 
     loop(1, C, sw_start)
-    dq_ring(4)
-    dq_ring(5)
-
-    def wr_wait(k):
-        at = block_of(k)
-        remote(s.wp.at[at], s.wr.at[at], s.wr_send.at[k], s.wr_recv.at[at], sp=at).wait_recv()
-
-    loop(1, Z, wr_wait)
-    s.wf[z] = lax.fori_loop(
-        1, Z, lambda i, a: a + s.wr[i].astype(f32), s.wr[0].astype(f32)
-    ).astype(bf16)
-
-    def wf_copy(k):
-        return remote(s.wf.at[z], s.wf.at[z], s.wf_send.at[k], s.wf_recv.at[z], sp=block_of(k))
-
-    loop(1, Z, lambda k: wf_copy(Z - k).start())
     dq_ring(6)
-
-    def sw_wait(k):
-        at = chip(k)
-        remote(s.sv.at[at], s.sw.at[at], s.sw_send.at[k], s.sw_recv.at[at], tp=other).wait_recv()
-
-    loop(1, C, sw_wait)
-    s.su8[...] = s.sw[0].astype(f32)
-
-    def add_sw(i):
-        s.su8[...] += s.sw[i].astype(f32)
-
-    loop(1, C, add_sw)
-    sgrad[...] = norm_back(s.src_scaled[...], s.src_inv[:, 0:1], sgain[...], s.su8[...])
+    w_relay()
     dq_ring(7)
     dq_ring(8)
+    w_owner()
     halves = []
     for sub in (0, 1):
         mine = s.dq[sub * hd : (sub + 1) * hd, own]
@@ -434,6 +457,11 @@
     tu_pair = remote(s.tsend, s.trecv, s.pair_send.at[1], s.pair_recv.at[1], tp=other)
     tu_pair.start()
     s.tmine[...] = nt(query_flat, half_cols(c)).reshape(C, TB, HALF)
+
+    def sw_wait(k):
+        at = chip(k)
+        remote(s.sv.at[at], s.sw.at[at], s.sw_send.at[k], s.sw_recv.at[at], tp=other).wait_recv()
+
     tu_pair.wait_recv()
 
     def tw_copy(k):
@@ -451,16 +479,38 @@
 
     loop(1, C, tw_start)
 
-    def wf_wait(k):
-        at = block_of(k)
-        remote(s.wf.at[at], s.wf.at[at], s.wf_send.at[k], s.wf_recv.at[at], sp=at).wait_recv()
-
-    loop(1, Z, wf_wait)
-
-    def put_weight(i):
-        wgrad[pl.ds(pl.multiple_of(i * CW, CW), CW), :] = s.wf[i].astype(f32).T
-
-    loop(0, Z, put_weight)
+    loop(1, C, sw_wait)
+    s.su8[...] = s.sw[0].astype(f32)
+
+    def add_sw(i):
+        s.su8[...] += s.sw[i].astype(f32)
+
+    loop(1, C, add_sw)
+    sgrad[...] = norm_back(s.src_scaled[...], s.src_inv[:, 0:1], sgain[...], s.su8[...])
+    f_relay()
+    loop(1, C, lambda k: source_copy(k).wait_send())
+    loop(0, C, lambda k: forward_copy(k).wait_send())
+    for way in (0, 1):
+        for step in range(1, H + 1):
+            block = zat(-(step - 1) if way == 0 else step - 1)
+            loop(*reach(way, step), lambda sub: ring_copy(block, sub, way, step).wait_send())
+    for k in range(1, G):
+        join_copy(k).wait_send()
+        dkv_copy(k).wait_send()
+
+    def line_sends(k):
+        stat_copy(k - 1).wait_send()
+        fin_copy(k).wait_send()
+
+    loop(1, Z, line_sends)
+    for way in (0, 1):
+        for sub in (0, 1):
+            for step in range(1, hops(way, sub) + 1):
+                dq_copy(way, step, sub).wait_send()
+        for k in range(1, top_hop[way] + 1):
+            w_copy(way, k).wait_send()
+    su_pair.wait_send()
+    loop(1, C, lambda k: sw_copy(k).wait_send())
 
     def tw_wait(k):
         at = chip(k)
@@ -493,34 +543,15 @@
     )
     tgrad[...] = cot + norm_back(scaled, inverse, tgain[...], upstream)
 
-    loop(1, C, lambda k: source_copy(k).wait_send())
-    loop(0, C, lambda k: forward_copy(k).wait_send())
+    for k in range(1, Z):
+        if k not in (2 * R - 1, 2 * R):
+            f_wait(k)
+    for i in range(Z):
+        wgrad[:, i * CW : (i + 1) * CW] = s.wf[i].astype(f32)
     for way in (0, 1):
-        for step in range(1, H + 1):
-            block = zat(-(step - 1) if way == 0 else step - 1)
-            loop(*reach(way, step), lambda sub: ring_copy(block, sub, way, step).wait_send())
-    for k in range(1, G):
-        join_copy(k).wait_send()
-        dkv_copy(k).wait_send()
-
-    def line_sends(k):
-        stat_copy(k).wait_send()
-        fin_copy(k).wait_send()
-        wr_copy(k).wait_send()
-        wf_copy(k).wait_send()
-
-    loop(1, Z, line_sends)
-    for way in (0, 1):
-        for sub in (0, 1):
-            for step in range(1, hops(way, sub) + 1):
-                dq_copy(way, step, sub).wait_send()
-
-    def plane_sends(k):
-        sw_copy(k).wait_send()
-        tw_copy(k).wait_send()
-
-    loop(1, C, plane_sends)
-    su_pair.wait_send()
+        for k in range(1, top_hop[way] + 1):
+            f_copy(way, k, k > R).wait_send()
+    loop(1, C, lambda k: tw_copy(k).wait_send())
     tu_pair.wait_send()
     last_pair.wait_send()
 
@@ -542,11 +573,11 @@
         dma = pltpu.SemaphoreType.DMA
         scratch = dict(
             src=V((SB, D), bf16), tgt=V((TR, D), bf16), cot=V((TR, D), bf16),
-            wq=V((D, HEAD), bf16), wk=V((D, PART), bf16), wv=V((D, PART), bf16), wo=V((HEAD, D), bf16),
+            wq=V((D, HEAD), bf16), wo=V((HEAD, D), bf16),
             t8=V((TB, D), bf16), c8=V((TB, D), bf16),
             src_scaled=V((SB, D), f32), src_inv=V((SB, 128), f32),
             g=V((T, SB, D), bf16), tn=V((TR, D), bf16), qd=V((Z * TR, 2 * HEAD), bf16),
-            wkv=V((D, 2 * PART), bf16), rows=V((SR, D), bf16), kvp=V((G, SR, 2 * PART), bf16),
+            wkv=V((2 * PART, D), bf16), rows=V((SR, D), bf16), kvp=V((G, SR, 2 * PART), bf16),
             keys=V((SR, HEAD), bf16), keys_t=V((HEAD, SR), bf16), values=V((SR, HEAD), bf16),
             e=V((Z, SR, TR), f32), p=V((Z, SR, TR), f32),
             stat=V((Z, 4, TR), f32), got=V((Z, 4, TR), f32), fin=V((Z, 2, TR), f32),
@@ -554,7 +585,8 @@
             dq_out=V((2, H + 1, 2, HEAD // 2, TR), bf16), dq_in=V((2, H + 1, 2, HEAD // 2, TR), bf16),
             dkv=V((G, SR, 2 * PART), f32), dkv_out=V((G, SR, 2 * PART), bf16), dkv_in=V((G, SR, 2 * PART), bf16),
             flat=V((SR, 2 * PART), bf16),
-            wp=V((Z, PART, CW), bf16), wr=V((Z, PART, CW), bf16), wf=V((Z, PART, CW), bf16),
+            wp=V((Z, PART, CW), bf16), w_in=V((2, H + 1, PART, CW), bf16), w_rel=V((2, PART, CW), bf16),
+            wf=V((Z, PART, CW), bf16),
             su=V((SR, D), f32), ss=V((C, SB, D), bf16), sr=V((C, SB, D), bf16),
             sv=V((C, SB, D), bf16), sw=V((C, SB, D), bf16), su8=V((SB, D), f32),
             tsend=V((C, TB, D // 2), bf16), trecv=V((C, TB, D // 2), bf16), tmine=V((C, TB, D // 2), f32),
@@ -564,19 +596,19 @@
             ring_send=dma((2, H + 1, SUBS)), ring_recv=dma((2, H + 1, SUBS)),
             join_send=dma((G,)), join_recv=dma((G,)), dkv_send=dma((G,)), dkv_recv=dma((G,)),
             stat_send=dma((Z,)), stat_recv=dma((Z,)), fin_send=dma((Z,)), fin_recv=dma((Z,)),
-            wr_send=dma((Z,)), wr_recv=dma((Z,)), wf_send=dma((Z,)), wf_recv=dma((Z,)),
+            w_send=dma((2, H + 1)), w_recv=dma((2, H + 1)), f_send=dma((2, H + 1)), f_recv=dma((Z,)),
             dq_send=dma((2, H + 1, 2)), dq_recv=dma((2, H + 1, 2)),
             sw_send=dma((C,)), sw_recv=dma((C,)), tw_send=dma((C,)), tw_recv=dma((C,)),
             pair_send=dma((3,)), pair_recv=dma((3,)),
         )
         vmem = pl.BlockSpec(memory_space=pltpu.VMEM)
         any_ = pl.BlockSpec(memory_space=pl.ANY)
-        return pl.pallas_call(
+        tgrad, sgrad, wgrad = pl.pallas_call(
             functools.partial(kernel, tuple(scratch), Z, T),
             out_shape=(
                 jax.ShapeDtypeStruct((TR // T, D), f32),
                 jax.ShapeDtypeStruct((SB, D), f32),
-                jax.ShapeDtypeStruct((D, PART), f32),
+                jax.ShapeDtypeStruct((PART, D), f32),
             ),
             in_specs=[any_, any_, any_, vmem, vmem, any_, any_, any_, any_],
             out_specs=(vmem, vmem, vmem),
@@ -585,7 +617,8 @@
                 collective_id=0, has_side_effects=True, vmem_limit_bytes=62 * 1024 * 1024
             ),
             name="backward",
-        )(target, source, cotangent, target_gain.reshape(1, D), source_gain.reshape(1, D), wq, wk, wv, wo)
+        )(target, source, cotangent, target_gain.reshape(1, D), source_gain.reshape(1, D), wq, wk.T, wv.T, wo)
+        return tgrad, sgrad, wgrad.T
 
     return jax.shard_map(
         on_device,

time: 135 us -> 109 us (0.81)
  Pallas kernels: 127 us -> 105 us
  local copies, waits for them, and re-layouts: 6.84 us -> 3.91 us
    pallas_call x1, Pallas kernels: 127 us -> 105 us  [on_device(): pl.pallas_call(functools.partial(kernel, tuple(scratch), Z, T), out_shape...]
    pallas_call x1 -> x0, local copies, waits for them, and re-layouts: 2.34 us -> none  [on_device(): pl.pallas_call(functools.partial(kernel, tuple(scratch), Z, T), out_shape...]
    unnamed x10 -> x5, local copies, waits for them, and re-layouts: 4.5 us -> 3.91 us
where the time goes in v2:
time: 109 us
  Pallas kernels  105 us (96%)
  local copies, waits for them, and re-layouts  3.91 us (4%)
    pallas_call x1, Pallas kernels, on_device(): pl.pallas_call(functools.partial(kernel, tuple(scratch), Z, T), out_shape...  105 us
    unnamed x5, local copies, waits for them, and re-layouts  3.91 us

profile of v2, /device:TPU:1, one launch (start us, length us, event | category | flops | bytes accessed | tf_op | source)
XLA Modules:
  0.0 109.2 jit_solution(1507541538897441716)
XLA Ops:
  0.6 104.7 %backward.1 = (f32[4,2048]{1,0:T(4,128)}, f32[8,2048]{1,0:T(8,128)}, f32[64,2048]{1,0:T(8,128)}) custom-call(bf16[128,2048]{1,0:T(8,128)(2,1)} %refs_0_.1, bf16[8,2048]{1,0:T(8,128)(2,1)} %refs_1_.1, bf16[128,2048]{1,0:T(8,128)(2,1)} %refs_2_.1, f32[1,2048]{1,0:T(1,128)} %bitcast.8, f32[1,2048]{1,0:T(1,128)} %bitcast.9, bf16[2048,256]{1,0:T(8,128)(2,1)} %refs_5_.1, ...), custom_call_target="tpu_custom_call" | custom-call | tf_op jit(solution)/shard_map/backward/pallas_call | solution.py:606
  105.3 0.0 copy-start
  105.3 1.4 %copy.15 = f32[4,2048]{1,0:T(4,128)} copy(f32[4,2048]{1,0:T(4,128)} %get-tuple-element.12) | data formatting | bytes 65536
  106.7 0.0 copy-done
  106.7 0.6 copy.16
  107.3 1.9 %copy.17 = f32[2048,64]{0,1:T(8,128)} copy(f32[2048,64]{0,1:T(8,128)} %bitcast.5) | data formatting | bytes 1048576
Async XLA Ops:
  105.3 1.4 %copy-start = (f32[8,2048]{1,0:T(8,128)S(1)}, f32[8,2048]{1,0:T(8,128)}, u32[]{:S(2)}) copy-start(f32[8,2048]{1,0:T(8,128)} %get-tuple-element.13) | copy-start | bytes 196612

commit v3 on v2

--- a/solution.py
+++ b/solution.py
@@ -14,7 +14,7 @@
 SCALE = HEAD**-0.5
 f32 = jnp.float32
 bf16 = jnp.bfloat16
-SUBS = 4
+SUBS = 8
 
 
 def nt(left, right):
@@ -163,13 +163,14 @@
                 ring_copy(block, sub, way, step + 1).start()
 
         def both(lo, hi, on):
-            def at(sub):
-                arrive(0, sub, on[0])
-                arrive(1, sub, on[1])
+            def at(pair):
+                for sub in (2 * pair, 2 * pair + 1):
+                    arrive(0, sub, on[0])
+                    arrive(1, sub, on[1])
                 if first >= 0:
-                    scores_sent(first + sub)
-
-            loop(lo, hi, at)
+                    scores_sent(first + pair)
+
+            loop(lo // 2, hi // 2, at)
 
         if step < H - 1:
             both(0, SUBS, (True, True))
@@ -181,9 +182,8 @@
             def last(sub):
                 arrive(0, sub, False)
                 arrive(1, SUBS // 2 + sub, False)
-                if first >= 0:
-                    scores_sent(first + sub)
-
+
+            loop(first, 2 * H - 1, scores_sent)
             loop(0, SUBS // 2, last)
 
     loads[5].wait()
@@ -206,6 +206,7 @@
         at = 2 * chip(k) + 1 - c
         remote(s.g.at[at], s.g.at[at], s.src_send.at[k], s.src_recv.at[at], tp=other).wait_recv()
 
+    ring(3)
     loop(0, C, from_other)
 
     def stack_rows(q):
@@ -220,17 +221,7 @@
 
     for k in range(1, G):
         join_copy(k).start()
-    ring(3)
     ring(4)
-    for k in range(1, G):
-        at = lax.rem(j + k, G)
-        remote(s.kvp.at[at], s.kvp.at[at], s.join_send.at[k], s.join_recv.at[at], tp=other).wait_recv()
-    parts = [s.kvp[i].astype(f32) for i in range(G)]
-    keys = jnp.concatenate([a[:, :PART] for a in parts], axis=1)
-    s.keys[...] = keys.astype(bf16)
-    s.keys_t[...] = keys.T.astype(bf16)
-    s.values[...] = jnp.concatenate([a[:, PART:] for a in parts], axis=1).astype(bf16)
-
     def block_of(k):
         return zat(lax.div(k + 1, 2) * (2 * lax.rem(k, 2) - 1))
 
@@ -256,11 +247,20 @@
         scores(k)
         stat_copy(k).start()
 
-    ring(5, 0)
-    ring(6, 4)
-    ring(7, 8)
+    ring(5)
+    for k in range(1, G):
+        at = lax.rem(j + k, G)
+        remote(s.kvp.at[at], s.kvp.at[at], s.join_send.at[k], s.join_recv.at[at], tp=other).wait_recv()
+    parts = [s.kvp[i].astype(f32) for i in range(G)]
+    keys = jnp.concatenate([a[:, :PART] for a in parts], axis=1)
+    s.keys[...] = keys.astype(bf16)
+    s.keys_t[...] = keys.T.astype(bf16)
+    s.values[...] = jnp.concatenate([a[:, PART:] for a in parts], axis=1).astype(bf16)
+    ring(6, 0)
+    loop(4, 6, scores_sent)
+    ring(7, 6)
+    loop(10, 12, scores_sent)
     ring(8, 12)
-    loop(14, 15, scores_sent)
     scores(15)
     far = zat(H)
     s.got[z] = s.stat[far]
@@ -270,15 +270,11 @@
         remote(s.stat.at[at], s.got.at[at], s.stat_send.at[k], s.stat_recv.at[at], sp=at).wait_recv()
 
     loop(1, Z, stat_wait)
-    top = lax.fori_loop(
-        1, Z, lambda i, a: jnp.maximum(a, s.got[i, 0:1, :]), s.got[0, 0:1, :]
-    )
-
-    def add_stats(i, sums):
-        factor = jnp.exp(s.got[i, 0:1, :] - top)
-        return sums[0] + s.got[i, 1:2, :] * factor, sums[1] + s.got[i, 2:3, :] * factor
-
-    total, weighted = lax.fori_loop(0, Z, add_stats, (jnp.zeros_like(top), jnp.zeros_like(top)))
+    parts = [s.got[i, 0:1, :] for i in range(Z)]
+    top = functools.reduce(jnp.maximum, parts)
+    factors = [jnp.exp(a - top) for a in parts]
+    total = sum(s.got[i, 1:2, :] * factors[i] for i in range(Z))
+    weighted = sum(s.got[i, 2:3, :] * factors[i] for i in range(Z))
     s.fin[far, 0:1, :] = top + jnp.log(total)
     s.fin[far, 1:2, :] = weighted / total
 
@@ -299,37 +295,48 @@
         s.att[:, cols] = weights.astype(bf16)
         s.slo[:, cols] = (weights * (s.p[b] - s.fin[b, 1:2, :]) * SCALE).astype(bf16)
 
-    loop(0, Z, slopes)
-    s.dq[...] = nn(s.keys_t[...], s.slo[...])
+    for k in range(2 * H - 3, 2 * H):
+        b = block_of(k)
+        slopes(b)
+        cols = pl.ds(pl.multiple_of(b * TR, TR), TR)
+        s.dq[:, cols] = nn(s.keys_t[...], s.slo[:, cols])
 
     hd = HEAD // 2
+    STEP = 2
+
+    def sign(way, k):
+        return zat(k if way == 1 else -k)
 
     def hops(way, sub):
         return H if way == sub else H - 1
 
-    def dq_copy(way, step, sub):
+    def dq_copy(way, k, sub):
         return remote(
-            s.dq_out.at[way, step, sub], s.dq_in.at[way, step, sub],
-            s.dq_send.at[way, step, sub], s.dq_recv.at[way, step, sub],
-            sp=zat(-1 if way == 0 else 1),
+            s.dq_out.at[way, k, sub], s.dq_in.at[way, k, sub],
+            s.dq_send.at[way, k, sub], s.dq_recv.at[way, k, sub],
+            sp=sign(way, k % STEP or STEP),
         )
 
-    def dq_ring(step):
+    def dq_sum(way, k, sub):
+        b = sign(way, k) if k else z
+        total = s.dq[sub * hd : (sub + 1) * hd, pl.ds(pl.multiple_of(b * TR, TR), TR)]
+        if k % STEP == 0:
+            for way_in in (way,) if k else (0, 1):
+                for far_k in range(k + 1, min(k + STEP, hops(way_in, sub)) + 1):
+                    dq_copy(way_in, far_k, sub).wait_recv()
+                    total = total + s.dq_in[way_in, far_k, sub].astype(f32)
+        return total
+
+    def dq_stage(k):
         for sub in (0, 1):
             for way in (0, 1):
-                if step > hops(way, sub):
-                    continue
-                far = hops(way, sub) + 1 - step
-                b = zat(-far if way == 0 else far)
-                mine = s.dq[sub * hd : (sub + 1) * hd, pl.ds(pl.multiple_of(b * TR, TR), TR)]
-                if step > 1:
-                    dq_copy(way, step - 1, sub).wait_recv()
-                    mine = mine + s.dq_in[way, step - 1, sub].astype(f32)
-                s.dq_out[way, step, sub] = mine.astype(bf16)
-                dq_copy(way, step, sub).start()
-
-    dq_ring(1)
-
+                if k <= hops(way, sub):
+                    s.dq_out[way, k, sub] = dq_sum(way, k, sub).astype(bf16)
+                    dq_copy(way, k, sub).start()
+
+    dq_stage(8)
+    dq_stage(7)
+    loop(0, 2 * H - 3, lambda k: slopes(block_of(k)))
     dk = nn(s.slo[...], s.qd[:, 0:HEAD])
     dv = nn(s.att[...], s.qd[:, HEAD : 2 * HEAD])
     for i in range(G):
@@ -343,8 +350,9 @@
 
     for k in range(1, G):
         dkv_copy(k).start()
-    dq_ring(2)
-    dq_ring(3)
+    s.dq[...] = nn(s.keys_t[...], s.slo[...])
+    dq_stage(6)
+    dq_stage(5)
     flat = s.dkv[j]
     for k in range(1, G):
         dkv_copy(k).wait_recv()
@@ -357,9 +365,6 @@
         s.wp[i] = part_t[:, i * CW : (i + 1) * CW].astype(bf16)
     R = H // 2
 
-    def sign(way, k):
-        return zat(k if way == 1 else -k)
-
     def w_copy(way, k):
         hop = k % R or R
         src = s.w_rel.at[way] if k == R else s.wp.at[sign(way, k)]
@@ -367,9 +372,8 @@
 
     top_hop = (2 * R, 2 * R - 1)
     for way in (0, 1):
-        for k in range(top_hop[way], 0, -1):
-            if k != R:
-                w_copy(way, k).start()
+        for k in range(top_hop[way], R, -1):
+            w_copy(way, k).start()
 
     def w_relay():
         for way in (0, 1):
@@ -406,7 +410,8 @@
             for k in range(top_hop[way], R, -1):
                 f_copy(way, k, True).start()
 
-    dq_ring(4)
+    dq_stage(4)
+    dq_stage(3)
     s.su[...] = nn(s.flat[...], s.wkv[...])
 
     def for_other(q):
@@ -415,7 +420,9 @@
     loop(0, C, for_other)
     su_pair = remote(s.ss, s.sr, s.pair_send.at[0], s.pair_recv.at[0], tp=other)
     su_pair.start()
-    dq_ring(5)
+    for way in (0, 1):
+        for k in range(R - 1, 0, -1):
+            w_copy(way, k).start()
     su_pair.wait_recv()
 
     def sw_copy(k):
@@ -433,20 +440,11 @@
         sw_copy(k).start()
 
     loop(1, C, sw_start)
-    dq_ring(6)
     w_relay()
-    dq_ring(7)
-    dq_ring(8)
+    dq_stage(2)
+    dq_stage(1)
     w_owner()
-    halves = []
-    for sub in (0, 1):
-        mine = s.dq[sub * hd : (sub + 1) * hd, own]
-        for way in (0, 1):
-            last = hops(way, sub)
-            dq_copy(way, last, sub).wait_recv()
-            mine = mine + s.dq_in[way, last, sub].astype(f32)
-        halves.append(mine)
-    query_flat = jnp.concatenate(halves, axis=0).T.astype(bf16)
+    query_flat = jnp.concatenate([dq_sum(0, 0, sub) for sub in (0, 1)], axis=0).T.astype(bf16)
 
     TB = TR // C
 
@@ -479,6 +477,7 @@
 
     loop(1, C, tw_start)
 
+    f_relay()
     loop(1, C, sw_wait)
     s.su8[...] = s.sw[0].astype(f32)
 
@@ -487,7 +486,6 @@
 
     loop(1, C, add_sw)
     sgrad[...] = norm_back(s.src_scaled[...], s.src_inv[:, 0:1], sgain[...], s.su8[...])
-    f_relay()
     loop(1, C, lambda k: source_copy(k).wait_send())
     loop(0, C, lambda k: forward_copy(k).wait_send())
     for way in (0, 1):
@@ -505,8 +503,8 @@
     loop(1, Z, line_sends)
     for way in (0, 1):
         for sub in (0, 1):
-            for step in range(1, hops(way, sub) + 1):
-                dq_copy(way, step, sub).wait_send()
+            for k in range(1, hops(way, sub) + 1):
+                dq_copy(way, k, sub).wait_send()
         for k in range(1, top_hop[way] + 1):
             w_copy(way, k).wait_send()
     su_pair.wait_send()
@@ -547,13 +545,19 @@
         if k not in (2 * R - 1, 2 * R):
             f_wait(k)
     for i in range(Z):
-        wgrad[:, i * CW : (i + 1) * CW] = s.wf[i].astype(f32)
+        wgrad[:, i * CW : (i + 1) * CW] = s.wf[i]
     for way in (0, 1):
         for k in range(1, top_hop[way] + 1):
             f_copy(way, k, k > R).wait_send()
     loop(1, C, lambda k: tw_copy(k).wait_send())
     tu_pair.wait_send()
     last_pair.wait_send()
+
+
+def put(tgrad, sgrad, wgrad, tgrad_out, sgrad_out, wgrad_out):
+    tgrad_out[...] = tgrad[...]
+    sgrad_out[...] = sgrad[...]
+    wgrad_out[...] = wgrad[...].astype(f32)
 
 
 def solution(mesh):
@@ -608,7 +612,7 @@
             out_shape=(
                 jax.ShapeDtypeStruct((TR // T, D), f32),
                 jax.ShapeDtypeStruct((SB, D), f32),
-                jax.ShapeDtypeStruct((PART, D), f32),
+                jax.ShapeDtypeStruct((PART, D), bf16),
             ),
             in_specs=[any_, any_, any_, vmem, vmem, any_, any_, any_, any_],
             out_specs=(vmem, vmem, vmem),
@@ -618,6 +622,17 @@
             ),
             name="backward",
         )(target, source, cotangent, target_gain.reshape(1, D), source_gain.reshape(1, D), wq, wk.T, wv.T, wo)
+        tgrad, sgrad, wgrad = pl.pallas_call(
+            put,
+            out_shape=(
+                jax.ShapeDtypeStruct((TR // T, D), f32),
+                jax.ShapeDtypeStruct((SB, D), f32),
+                jax.ShapeDtypeStruct((PART, D), f32),
+            ),
+            in_specs=[vmem, vmem, vmem],
+            out_specs=(vmem, vmem, vmem),
+            name="put",
+        )(tgrad, sgrad, wgrad)
         return tgrad, sgrad, wgrad.T
 
     return jax.shard_map(

time: 109 us -> 101 us (0.927)
  Pallas kernels: 105 us -> 101 us
  local copies, waits for them, and re-layouts: 3.91 us -> 0 us
    pallas_call x1, Pallas kernels: 105 us -> 98.7 us  [on_device(): pl.pallas_call(functools.partial(kernel, tuple(scratch), Z, T), out_shape...]
    unnamed x5 -> x0, local copies, waits for them, and re-layouts: 3.91 us -> none
    pallas_call x0 -> x1, Pallas kernels: none -> 1.85 us  [on_device(): pl.pallas_call(put, out_shape=(jax.ShapeDtypeStruct((TR // T, D), f32), j...]
where the time goes in v3:
time: 101 us
  Pallas kernels  101 us (100%)
    pallas_call x1, Pallas kernels, on_device(): pl.pallas_call(functools.partial(kernel, tuple(scratch), Z, T), out_shape...  98.7 us

profile of v3, /device:TPU:1, one launch (start us, length us, event | category | flops | bytes accessed | tf_op | source)
XLA Modules:
  0.0 101.2 jit_solution(14349868043968827318)
XLA Ops:
  0.6 98.7 %backward.1 = (f32[4,2048]{1,0:T(4,128)}, f32[8,2048]{1,0:T(8,128)}, bf16[64,2048]{1,0:T(8,128)(2,1)}) custom-call(bf16[128,2048]{1,0:T(8,128)(2,1)} %refs_0_.1, bf16[8,2048]{1,0:T(8,128)(2,1)} %refs_1_.1, bf16[128,2048]{1,0:T(8,128)(2,1)} %refs_2_.1, f32[1,2048]{1,0:T(1,128)} %bitcast.7, f32[1,2048]{1,0:T(1,128)} %bitcast.8, bf16[2048,256]{1,0:T(8,128)(2,1)} %refs_5_.1, ...), custom_call_target="tpu_custom_call" | custom-call | tf_op jit(solution)/shard_map/backward/pallas_call | solution.py:610
  99.3 1.8 %put.1 = (f32[4,2048]{1,0:T(4,128)}, f32[8,2048]{1,0:T(8,128)}, f32[64,2048]{1,0:T(8,128)}) custom-call(f32[4,2048]{1,0:T(4,128)} %get-tuple-element.9.tgrad, f32[8,2048]{1,0:T(8,128)} %get-tuple-element.10.sgrad, bf16[64,2048]{1,0:T(8,128)(2,1)} %get-tuple-element.11.wgrad), custom_call_target="tpu_custom_call" | custom-call | tf_op jit(solution)/shard_map/put/pallas_call | solution.py:625

commit v4 on v3

--- a/solution.py
+++ b/solution.py
@@ -199,8 +199,9 @@
         row = s.g.at[same(k)]
         return remote(row, row, s.src_send.at[k], s.src_recv.at[same(k)], tp=other)
 
-    loop(1, C, pass_on)
+    loop(1, C // 2, pass_on)
     ring(2)
+    loop(C // 2, C, pass_on)
 
     def from_other(k):
         at = 2 * chip(k) + 1 - c
@@ -284,22 +285,14 @@
     loop(1, Z, lambda k: fin_copy(Z - k).start())
 
     def fin_wait(k):
-        at = block_of(k - 1)
+        at = block_of(k)
         remote(s.fin.at[at], s.fin.at[at], s.fin_send.at[k], s.fin_recv.at[at], sp=at).wait_recv()
-
-    loop(1, Z, fin_wait)
 
     def slopes(b):
         cols = pl.ds(pl.multiple_of(b * TR, TR), TR)
         weights = s.e[b] * jnp.exp(s.stat[b, 0:1, :] - s.fin[b, 0:1, :])
         s.att[:, cols] = weights.astype(bf16)
         s.slo[:, cols] = (weights * (s.p[b] - s.fin[b, 1:2, :]) * SCALE).astype(bf16)
-
-    for k in range(2 * H - 3, 2 * H):
-        b = block_of(k)
-        slopes(b)
-        cols = pl.ds(pl.multiple_of(b * TR, TR), TR)
-        s.dq[:, cols] = nn(s.keys_t[...], s.slo[:, cols])
 
     hd = HEAD // 2
     STEP = 2
@@ -334,9 +327,28 @@
                     s.dq_out[way, k, sub] = dq_sum(way, k, sub).astype(bf16)
                     dq_copy(way, k, sub).start()
 
+    def settle(k):
+        fin_wait(k)
+        slopes(block_of(k))
+
+    def part(k):
+        cols = pl.ds(pl.multiple_of(block_of(k) * TR, TR), TR)
+        s.dq[:, cols] = nn(s.keys_t[...], s.slo[:, cols])
+
+    slopes(far)
+    part(2 * H - 1)
     dq_stage(8)
+    for k in (13, 14):
+        settle(k)
+        part(k)
     dq_stage(7)
-    loop(0, 2 * H - 3, lambda k: slopes(block_of(k)))
+    for k in (11, 12, 9, 10):
+        settle(k)
+        part(k)
+    dq_stage(5)
+    loop(0, 4, lambda i: settle(8 - i))
+    dq_stage(6)
+    loop(0, 5, lambda i: settle(4 - i))
     dk = nn(s.slo[...], s.qd[:, 0:HEAD])
     dv = nn(s.att[...], s.qd[:, HEAD : 2 * HEAD])
     for i in range(G):
@@ -351,8 +363,8 @@
     for k in range(1, G):
         dkv_copy(k).start()
     s.dq[...] = nn(s.keys_t[...], s.slo[...])
-    dq_stage(6)
-    dq_stage(5)
+    dq_stage(3)
+    dq_stage(4)
     flat = s.dkv[j]
     for k in range(1, G):
         dkv_copy(k).wait_recv()
@@ -410,8 +422,7 @@
             for k in range(top_hop[way], R, -1):
                 f_copy(way, k, True).start()
 
-    dq_stage(4)
-    dq_stage(3)
+    dq_stage(1)
     s.su[...] = nn(s.flat[...], s.wkv[...])
 
     def for_other(q):
@@ -423,6 +434,7 @@
     for way in (0, 1):
         for k in range(R - 1, 0, -1):
             w_copy(way, k).start()
+    dq_stage(2)
     su_pair.wait_recv()
 
     def sw_copy(k):
@@ -441,9 +453,6 @@
 
     loop(1, C, sw_start)
     w_relay()
-    dq_stage(2)
-    dq_stage(1)
-    w_owner()
     query_flat = jnp.concatenate([dq_sum(0, 0, sub) for sub in (0, 1)], axis=0).T.astype(bf16)
 
     TB = TR // C
@@ -460,6 +469,7 @@
         at = chip(k)
         remote(s.sv.at[at], s.sw.at[at], s.sw_send.at[k], s.sw_recv.at[at], tp=other).wait_recv()
 
+    w_owner()
     tu_pair.wait_recv()
 
     def tw_copy(k):
@@ -477,7 +487,6 @@
 
     loop(1, C, tw_start)
 
-    f_relay()
     loop(1, C, sw_wait)
     s.su8[...] = s.sw[0].astype(f32)
 
@@ -486,6 +495,7 @@
 
     loop(1, C, add_sw)
     sgrad[...] = norm_back(s.src_scaled[...], s.src_inv[:, 0:1], sgain[...], s.su8[...])
+    f_relay()
     loop(1, C, lambda k: source_copy(k).wait_send())
     loop(0, C, lambda k: forward_copy(k).wait_send())
     for way in (0, 1):

time: 101 us -> 96.1 us (0.951)
  Pallas kernels: 101 us -> 95.3 us
    pallas_call x1, Pallas kernels: 98.7 us -> 93.4 us  [on_device(): pl.pallas_call(functools.partial(kernel, tuple(scratch), Z, T), out_shape...]
where the time goes in v4:
time: 96.1 us; the launch traced here: 95.9 us
  Pallas kernels  95.3 us (99%)
    pallas_call x1, Pallas kernels, on_device(): pl.pallas_call(functools.partial(kernel, tuple(scratch), Z, T), out_shape...  93.4 us

profile of v4, /device:TPU:1, one launch (start us, length us, event | category | flops | bytes accessed | tf_op | source)
XLA Modules:
  0.0 95.9 jit_solution(210473144016699008)
XLA Ops:
  0.6 93.4 %backward.1 = (f32[4,2048]{1,0:T(4,128)}, f32[8,2048]{1,0:T(8,128)}, bf16[64,2048]{1,0:T(8,128)(2,1)}) custom-call(bf16[128,2048]{1,0:T(8,128)(2,1)} %refs_0_.1, bf16[8,2048]{1,0:T(8,128)(2,1)} %refs_1_.1, bf16[128,2048]{1,0:T(8,128)(2,1)} %refs_2_.1, f32[1,2048]{1,0:T(1,128)} %bitcast.7, f32[1,2048]{1,0:T(1,128)} %bitcast.8, bf16[2048,256]{1,0:T(8,128)(2,1)} %refs_5_.1, ...), custom_call_target="tpu_custom_call" | custom-call | tf_op jit(solution)/shard_map/backward/pallas_call | solution.py:620
  94.1 1.8 %put.1 = (f32[4,2048]{1,0:T(4,128)}, f32[8,2048]{1,0:T(8,128)}, f32[64,2048]{1,0:T(8,128)}) custom-call(f32[4,2048]{1,0:T(4,128)} %get-tuple-element.9.tgrad, f32[8,2048]{1,0:T(8,128)} %get-tuple-element.10.sgrad, bf16[64,2048]{1,0:T(8,128)(2,1)} %get-tuple-element.11.wgrad), custom_call_target="tpu_custom_call" | custom-call | tf_op jit(solution)/shard_map/put/pallas_call | solution.py:635

commit v5 on v4

--- a/solution.py
+++ b/solution.py
@@ -349,29 +349,33 @@
     loop(0, 4, lambda i: settle(8 - i))
     dq_stage(6)
     loop(0, 5, lambda i: settle(4 - i))
-    dk = nn(s.slo[...], s.qd[:, 0:HEAD])
-    dv = nn(s.att[...], s.qd[:, HEAD : 2 * HEAD])
-    for i in range(G):
-        cut = slice(i * PART, (i + 1) * PART)
-        s.dkv[i] = jnp.concatenate((dk[:, cut], dv[:, cut]), axis=1)
-    for k in range(1, G):
-        s.dkv_out[k] = s.dkv[lax.rem(j + k, G)].astype(bf16)
-
-    def dkv_copy(k):
-        return remote(s.dkv_out.at[k], s.dkv_in.at[k], s.dkv_send.at[k], s.dkv_recv.at[k], tp=mate(k))
-
-    for k in range(1, G):
-        dkv_copy(k).start()
+    def share(i):
+        return pl.ds(pl.multiple_of(i * PART, PART), PART)
+
+    def dkv_copy(h, k):
+        return remote(
+            s.dkv_out.at[h, k], s.dkv_in.at[h, k], s.dkv_send.at[h, k], s.dkv_recv.at[h, k], tp=mate(k)
+        )
+
+    for h, left in enumerate((s.slo, s.att)):
+        s.dkv[h] = nn(left[...], s.qd[:, h * HEAD : (h + 1) * HEAD]).T
+        for k in range(1, G):
+            s.dkv_out[h, k] = s.dkv[h, share(lax.rem(j + k, G)), :].astype(bf16)
+        for k in range(1, G):
+            dkv_copy(h, k).start()
+
+    def group_sum(h):
+        total = s.dkv[h, share(j), :]
+        for k in range(1, G):
+            dkv_copy(h, k).wait_recv()
+            total = total + s.dkv_in[h, k].astype(f32)
+        return total
+
     s.dq[...] = nn(s.keys_t[...], s.slo[...])
     dq_stage(3)
     dq_stage(4)
-    flat = s.dkv[j]
-    for k in range(1, G):
-        dkv_copy(k).wait_recv()
-        flat = flat + s.dkv_in[k].astype(f32)
-    s.flat[...] = flat.astype(bf16)
-
-    part_t = nn(flat.T[:PART, :].astype(bf16), s.rows[...])
+    keys_part = group_sum(0)
+    part_t = nn(keys_part.astype(bf16), s.rows[...])
     CW = D // Z
     for i in range(Z):
         s.wp[i] = part_t[:, i * CW : (i + 1) * CW].astype(bf16)
@@ -423,6 +427,7 @@
                 f_copy(way, k, True).start()
 
     dq_stage(1)
+    s.flat[...] = jnp.concatenate((keys_part, group_sum(1)), axis=0).T.astype(bf16)
     s.su[...] = nn(s.flat[...], s.wkv[...])
 
     def for_other(q):
@@ -431,10 +436,10 @@
     loop(0, C, for_other)
     su_pair = remote(s.ss, s.sr, s.pair_send.at[0], s.pair_recv.at[0], tp=other)
     su_pair.start()
+    dq_stage(2)
     for way in (0, 1):
         for k in range(R - 1, 0, -1):
             w_copy(way, k).start()
-    dq_stage(2)
     su_pair.wait_recv()
 
     def sw_copy(k):
@@ -504,7 +509,8 @@
             loop(*reach(way, step), lambda sub: ring_copy(block, sub, way, step).wait_send())
     for k in range(1, G):
         join_copy(k).wait_send()
-        dkv_copy(k).wait_send()
+        dkv_copy(0, k).wait_send()
+        dkv_copy(1, k).wait_send()
 
     def line_sends(k):
         stat_copy(k - 1).wait_send()
@@ -597,7 +603,7 @@
             stat=V((Z, 4, TR), f32), got=V((Z, 4, TR), f32), fin=V((Z, 2, TR), f32),
             att=V((SR, Z * TR), bf16), slo=V((SR, Z * TR), bf16), dq=V((HEAD, Z * TR), f32),
             dq_out=V((2, H + 1, 2, HEAD // 2, TR), bf16), dq_in=V((2, H + 1, 2, HEAD // 2, TR), bf16),
-            dkv=V((G, SR, 2 * PART), f32), dkv_out=V((G, SR, 2 * PART), bf16), dkv_in=V((G, SR, 2 * PART), bf16),
+            dkv=V((2, HEAD, SR), f32), dkv_out=V((2, G, PART, SR), bf16), dkv_in=V((2, G, PART, SR), bf16),
             flat=V((SR, 2 * PART), bf16),
             wp=V((Z, PART, CW), bf16), w_in=V((2, H + 1, PART, CW), bf16), w_rel=V((2, PART, CW), bf16),
             wf=V((Z, PART, CW), bf16),
@@ -608,7 +614,7 @@
             tx_out=V((TB // 2, D // 2), f32), tx_in=V((TB // 2, D // 2), f32),
             in_sem=dma((9,)), src_send=dma((C,)), fwd_send=dma((C,)), src_recv=dma((T,)),
             ring_send=dma((2, H + 1, SUBS)), ring_recv=dma((2, H + 1, SUBS)),
-            join_send=dma((G,)), join_recv=dma((G,)), dkv_send=dma((G,)), dkv_recv=dma((G,)),
+            join_send=dma((G,)), join_recv=dma((G,)), dkv_send=dma((2, G)), dkv_recv=dma((2, G)),
             stat_send=dma((Z,)), stat_recv=dma((Z,)), fin_send=dma((Z,)), fin_recv=dma((Z,)),
             w_send=dma((2, H + 1)), w_recv=dma((2, H + 1)), f_send=dma((2, H + 1)), f_recv=dma((Z,)),
             dq_send=dma((2, H + 1, 2)), dq_recv=dma((2, H + 1, 2)),

time: 96.1 us -> 96.9 us (level)
  no operation moved by 1% of the time
where the time goes in v5:
time: 96.9 us; the launch traced here: 96.1 us
  Pallas kernels  95.5 us (99%)
    pallas_call x1, Pallas kernels, on_device(): pl.pallas_call(functools.partial(kernel, tuple(scratch), Z, T), out_shape...  93.6 us

profile of v5, /device:TPU:1, one launch (start us, length us, event | category | flops | bytes accessed | tf_op | source)
XLA Modules:
  0.0 96.1 jit_solution(12813134019298763348)
XLA Ops:
  0.6 93.6 %backward.1 = (f32[4,2048]{1,0:T(4,128)}, f32[8,2048]{1,0:T(8,128)}, bf16[64,2048]{1,0:T(8,128)(2,1)}) custom-call(bf16[128,2048]{1,0:T(8,128)(2,1)} %refs_0_.1, bf16[8,2048]{1,0:T(8,128)(2,1)} %refs_1_.1, bf16[128,2048]{1,0:T(8,128)(2,1)} %refs_2_.1, f32[1,2048]{1,0:T(1,128)} %bitcast.7, f32[1,2048]{1,0:T(1,128)} %bitcast.8, bf16[2048,256]{1,0:T(8,128)(2,1)} %refs_5_.1, ...), custom_call_target="tpu_custom_call" | custom-call | tf_op jit(solution)/shard_map/backward/pallas_call | solution.py:626
  94.3 1.8 %put.1 = (f32[4,2048]{1,0:T(4,128)}, f32[8,2048]{1,0:T(8,128)}, f32[64,2048]{1,0:T(8,128)}) custom-call(f32[4,2048]{1,0:T(4,128)} %get-tuple-element.9.tgrad, f32[8,2048]{1,0:T(8,128)} %get-tuple-element.10.sgrad, bf16[64,2048]{1,0:T(8,128)(2,1)} %get-tuple-element.11.wgrad), custom_call_target="tpu_custom_call" | custom-call | tf_op jit(solution)/shard_map/put/pallas_call | solution.py:641
